TPU v7x, 32 devices: a whole 2x2x4 slice. The times are simulated.
32 devices in a mesh: sp: 4 (over z), fs: 2 (over y), tp: 4 (over x, core).
Axes of the slice: x: 2, y: 2, z: 4, core: 2. Of those that a mesh axis runs over, the one named last changes fastest.
Arguments:
- tokens: bfloat16 [2, 3072, 2304], P('fs', 'sp'), may hold values from -6 to 6
- norm_gain: float32 [2304], replicated, may hold values from 0.1 to 1.9
- query_weight: bfloat16 [2304, 2048], P(('sp', 'fs'), 'tp'), may hold values from -6 to 6
- key_weight: bfloat16 [2304, 512], P(('sp', 'fs'), 'tp'), may hold values from -6 to 6
- value_weight: bfloat16 [2304, 512], P(('sp', 'fs'), 'tp'), may hold values from -0.125 to 0.125
- outer_weight: bfloat16 [2304, 2048], P(('sp', 'fs'), 'tp'), may hold values from -0.125 to 0.125
- inner_weight: bfloat16 [2304, 2048], P(('sp', 'fs'), 'tp'), may hold values from -0.125 to 0.125
- signal_weight: bfloat16 [2304, 2048], P(('sp', 'fs'), 'tp'), may hold values from -0.125 to 0.125
- conv_taps: float32 [3, 2048], P(None, 'tp'), may hold values from -3 to 3
- sink_logit: float32 [32], P('tp'), may hold values from -4 to 4
Outputs:
- attn_out: bfloat16 [2, 3072, 2048], P('fs', 'sp', 'tp')
- conv_out: bfloat16 [2, 3072, 2048], P('fs', 'sp', 'tp')
- log_total: float32 [2, 32, 3072], P('fs', 'tp', 'sp')
All inputs are finite; a program needn't handle non-finite values.
Results may differ from a plain program's by a relative error of at most 0.014.
The roundings to bfloat16 on the way count: a program that leaves them out, or rounds other values in their place, can miss the bound.
Values may be sent and summed in bfloat16 or wider, within the bound.
A program may use at most 64 MiB of HBM per device.

v0:
```python
import math

import functools

import jax
import jax.numpy as jnp
from jax import lax
from jax.experimental import pallas as pl
from jax.experimental.pallas import tpu as pltpu
from jax.sharding import PartitionSpec as P

HEAD = 64
WINDOW = 128


EPSILON = 1e-06


def extended(value, sides, width):
    for axis, dim in sides:
        size, length = (lax.axis_size(axis), value.shape[dim])
        up = [(i, (i + 1) % size) for i in range(size - 1)]
        down = [(j, i) for i, j in up]
        last = lax.slice_in_dim(value, length - width, length, axis=dim)
        initial = lax.slice_in_dim(value, 0, width, axis=dim)
        before = lax.ppermute(last, axis, up)
        after = lax.ppermute(initial, axis, down)
        value = jnp.concatenate([before, value, after], axis=dim)
    return value


def normalized(tokens, norm_gain):
    values = tokens.astype(jnp.float32)
    scaling = lax.rsqrt(jnp.mean(values * values, axis=-1, keepdims=True) + EPSILON)
    return (values * scaling * norm_gain).astype(jnp.bfloat16)


def folding(normed):

    def add_portions(running, portions, offset):
        return tuple(
            (jnp.dot(normed, portion, preferred_element_type=jnp.float32) for portion in portions)
        )

    return add_portions


def empty_sums(normed, weights):
    return tuple((jnp.zeros((normed.shape[0], weight.shape[1]), jnp.float32) for weight in weights))


def rounded(results):
    return tuple((result.astype(jnp.bfloat16) for result in results))


def gate_product(inner_gate, signal):
    return (inner_gate.astype(jnp.float32) * signal.astype(jnp.float32)).astype(jnp.bfloat16)


def send_edges(key_proj, value_proj, product):
    stacked = jnp.concatenate([key_proj, value_proj], axis=1)
    window_rows = extended(stacked, (("sp", 0),), WINDOW)
    conv_rows = extended(product, (("sp", 0),), 1)
    return (window_rows, conv_rows)


def banded_attention(queries, window_rows, sink_logit, slopes, first_pos, seq_length):
    tok_count = queries.shape[0]
    kv_cols = window_rows.shape[1] // 2
    kv_heads = kv_cols // HEAD
    group_size = queries.shape[1] // (HEAD * kv_heads)
    block_count = tok_count // WINDOW
    query_blocks = queries.reshape(block_count, WINDOW, kv_heads, group_size, HEAD)
    key_rows = window_rows[:, :kv_cols].reshape(block_count + 2, WINDOW, kv_heads, HEAD)
    value_rows = window_rows[:, kv_cols:].reshape(block_count + 2, WINDOW, kv_heads, HEAD)
    key_span = jnp.concatenate([key_rows[:-2], key_rows[1:-1], key_rows[2:]], axis=1)
    value_span = jnp.concatenate([value_rows[:-2], value_rows[1:-1], value_rows[2:]], axis=1)
    scores = jnp.einsum(
        "bqkgd,bskd->bkgqs", query_blocks, key_span, preferred_element_type=jnp.float32
    ) * (1.0 / math.sqrt(HEAD))
    distance = jnp.arange(WINDOW)[:, None] - jnp.arange(3 * WINDOW)[None, :] + WINDOW
    key_pos = (
        first_pos
        - WINDOW
        + WINDOW * jnp.arange(block_count)[:, None]
        + jnp.arange(3 * WINDOW)[None, :]
    )
    inside = (jnp.abs(distance)[None] <= WINDOW) & ((key_pos >= 0) & (key_pos < seq_length))[
        :, None, :
    ]
    scores = scores - slopes.reshape(kv_heads, group_size, 1, 1) * jnp.abs(distance).astype(
        jnp.float32
    )
    scores = jnp.where(inside[:, None, None], scores, -jnp.inf)
    sink_grid = sink_logit.reshape(kv_heads, group_size, 1, 1)
    row_peak = jnp.maximum(jnp.max(scores, axis=-1, keepdims=True), sink_grid)
    weights = jnp.exp(scores - row_peak)
    row_total = jnp.sum(weights, axis=-1, keepdims=True) + jnp.exp(sink_grid - row_peak)
    weighted = jnp.einsum(
        "bkgqs,bskd->bqkgd",
        weights.astype(jnp.bfloat16),
        value_span,
        preferred_element_type=jnp.float32,
    )
    attended = (
        (weighted / row_total.transpose(0, 3, 1, 2, 4))
        .astype(jnp.bfloat16)
        .reshape(tok_count, kv_heads * group_size * HEAD)
    )
    log_total = (
        (row_peak + jnp.log(row_total))[..., 0]
        .transpose(1, 2, 0, 3)
        .reshape(kv_heads * group_size, tok_count)
    )
    return (attended, log_total)


def per_device(
    tokens,
    norm_gain,
    query_weight,
    key_weight,
    value_weight,
    outer_weight,
    inner_weight,
    signal_weight,
    conv_taps,
    sink_logit,
):
    normed = normalized(tokens[0], norm_gain)
    add_portions = folding(normed)
    all_sums = add_portions(
        empty_sums(
            normed,
            (query_weight, key_weight, value_weight, outer_weight, inner_weight, signal_weight),
        ),
        (
            lax.all_gather(query_weight, ("sp", "fs"), axis=0, tiled=True),
            lax.all_gather(key_weight, ("sp", "fs"), axis=0, tiled=True),
            lax.all_gather(value_weight, ("sp", "fs"), axis=0, tiled=True),
            lax.all_gather(outer_weight, ("sp", "fs"), axis=0, tiled=True),
            lax.all_gather(inner_weight, ("sp", "fs"), axis=0, tiled=True),
            lax.all_gather(signal_weight, ("sp", "fs"), axis=0, tiled=True),
        ),
        jnp.int32(0),
    )
    queries, key_proj, value_proj, outer_gate, inner_gate, signal = rounded(all_sums)
    product = gate_product(inner_gate, signal)
    window_rows, conv_rows = send_edges(key_proj, value_proj, product)
    tok_count = normed.shape[0]
    head_local = queries.shape[1] // HEAD
    head_index = lax.axis_index("tp") * head_local + jnp.arange(1, head_local + 1)
    slopes = jnp.exp2(-8.0 * head_index.astype(jnp.float32) / (head_local * lax.axis_size("tp")))
    first_pos = lax.axis_index("sp") * tok_count
    attended, log_total = banded_attention(
        queries, window_rows, sink_logit, slopes, first_pos, tok_count * lax.axis_size("sp")
    )
    mixed_conv = conv_taps[0] * conv_rows[0:tok_count].astype(jnp.float32)
    mixed_conv = mixed_conv + conv_taps[1] * conv_rows[1 : tok_count + 1].astype(jnp.float32)
    mixed_conv = mixed_conv + conv_taps[2] * conv_rows[2 : tok_count + 2].astype(jnp.float32)
    conv_out = (outer_gate.astype(jnp.float32) * mixed_conv).astype(jnp.bfloat16)
    return (attended[None], conv_out[None], log_total[None])


MESH = pl.DeviceIdType.MESH
GROUPS = 3
FAR = -1e30


def mega_kernel(
    ns,
    tokens,
    gain,
    qw,
    kvw,
    ow,
    iw,
    sw,
    taps,
    slopes,
    sinks,
    attn_out,
    conv_out,
    log_out,
    toks,
    wts,
    stage_w,
    qs,
    kvs,
    bias,
    prod,
    outer,
    attn_st,
    log_st,
    conv_st,
    load_sem,
    stage_sem,
    misc_sem,
    y_send,
    w_recv,
    up_send,
    dn_send,
    tok_send,
    tok_recv,
    kv_send,
    kv_recv,
    pr_send,
    pr_recv,
    ret_send,
    ret_recv,
):
    s, f, t = lax.axis_index("sp"), lax.axis_index("fs"), lax.axis_index("tp")
    other = 1 - f
    core = lax.rem(t, 2)
    mate = t + 1 - 2 * core
    rows = tokens.shape[0]
    half_rows = rows // 2
    depth = qw.shape[0]
    qcols = qs.shape[2]
    heads = qcols // HEAD
    chans = prod.shape[3]
    blocks = rows // WINDOW
    pad = (prod.shape[2] - rows) // 2
    up, down, across, beside = (s + 1, f, t), (s - 1, f, t), (s, other, t), (s, f, mate)
    has_up, has_down = s < ns - 1, s > 0

    barrier = pltpu.get_barrier_semaphore()

    @pl.when(has_up)
    def _():
        pl.semaphore_signal(barrier, inc=1, device_id=up, device_id_type=MESH)

    @pl.when(has_down)
    def _():
        pl.semaphore_signal(barrier, inc=1, device_id=down, device_id_type=MESH)

    pl.semaphore_signal(barrier, inc=1, device_id=across, device_id_type=MESH)
    pl.semaphore_signal(barrier, inc=1, device_id=beside, device_id_type=MESH)

    def block_rows(blk):
        return pl.ds(pl.multiple_of(blk * depth, 16), depth)

    def loads(g, half, dest, sems):
        if g == 0:
            qc = pl.ds(pl.multiple_of(half * qcols, 128), qcols)
            pairs = [
                (qw.at[:, qc], dest.at[:, pl.ds(0, qcols)]),
                (kvw.at[half], dest.at[:, pl.ds(qcols, 2 * HEAD)]),
            ]
        else:
            c = pl.ds(pl.multiple_of(half * (2 * chans) + (g - 1) * chans, 128), chans)
            pairs = [
                (ref.at[:, c], dest.at[:, pl.ds(i * chans, chans)])
                for i, ref in enumerate((iw, sw, ow))
            ]
        return [
            pltpu.make_async_copy(a, b, sems.at[g, i]) for i, (a, b) in enumerate(pairs)
        ]

    mine = s * 2 + f
    theirs = s * 2 + other
    own_loads = [loads(g, f, wts.at[g, block_rows(mine)], load_sem) for g in range(GROUPS)]
    out_loads = [loads(g, other, stage_w.at[g], stage_sem) for g in range(GROUPS)]
    for g in range(GROUPS):
        for c in out_loads[g] + own_loads[g]:
            c.start()
    tok_load = pltpu.make_async_copy(tokens, toks.at[f], misc_sem.at[0])
    tok_load.start()

    pl.semaphore_wait(
        barrier, 2 + jnp.where(has_up, 1, 0) + jnp.where(has_down, 1, 0)
    )

    y_copies = []
    for g in range(GROUPS):
        for c in out_loads[g]:
            c.wait()
        copy = pltpu.make_async_remote_copy(
            src_ref=stage_w.at[g],
            dst_ref=wts.at[g, block_rows(mine)],
            send_sem=y_send.at[g],
            recv_sem=w_recv.at[g, mine],
            device_id=across,
            device_id_type=MESH,
        )
        copy.start()
        y_copies.append(copy)
        for c in own_loads[g]:
            c.wait()
    share = pl.ds(pl.multiple_of(core * half_rows, 16), half_rows)
    rest = pl.ds(pl.multiple_of((1 - core) * half_rows, 16), half_rows)
    tok_copy = pltpu.make_async_remote_copy(
        src_ref=tokens.at[share],
        dst_ref=toks.at[f, share],
        send_sem=tok_send.at[0],
        recv_sem=tok_recv.at[0],
        device_id=across,
        device_id_type=MESH,
    )
    tok_copy.start()

    def incoming(g, blk):
        return pltpu.make_async_remote_copy(
            src_ref=wts.at[g, block_rows(blk)],
            dst_ref=wts.at[g, block_rows(blk)],
            send_sem=up_send.at[g, blk],
            recv_sem=w_recv.at[g, blk],
            device_id=across,
            device_id_type=MESH,
        )

    def forward(g, blk, upward):
        return pltpu.make_async_remote_copy(
            src_ref=wts.at[g, block_rows(blk)],
            dst_ref=wts.at[g, block_rows(blk)],
            send_sem=(up_send if upward else dn_send).at[g, blk],
            recv_sem=w_recv.at[g, blk],
            device_id=up if upward else down,
            device_id_type=MESH,
        )

    def relay_step(g, d, par):
        side = f if par == 0 else other
        if d == 0:
            blk = s * 2 + side
            if par == 1:
                incoming(g, blk).wait_recv()

            @pl.when(has_up)
            def _():
                forward(g, blk, True).start()

            @pl.when(has_down)
            def _():
                forward(g, blk, False).start()

            return

        @pl.when(s - d >= 0)
        def _():
            blk = (s - d) * 2 + side
            incoming(g, blk).wait_recv()

            @pl.when(has_up)
            def _():
                forward(g, blk, True).start()

        @pl.when(s + d < ns)
        def _():
            blk = (s + d) * 2 + side
            incoming(g, blk).wait_recv()

            @pl.when(has_down)
            def _():
                forward(g, blk, False).start()

    def settle():
        for g in range(GROUPS):
            y_copies[g].wait_send()
            for d in range(ns):
                for par in range(2):
                    side = f if par == 0 else other

                    @pl.when((s - d >= 0) & has_up)
                    def _():
                        forward(g, (s - d) * 2 + side, True).wait_send()

                    @pl.when((s + d < ns) & has_down)
                    def _():
                        forward(g, (s + d) * 2 + side, False).wait_send()

    def norm_rows(seq):
        @pl.loop(0, blocks)
        def _(b):
            at = pl.ds(pl.multiple_of(b * WINDOW, WINDOW), WINDOW)
            values = toks[seq, at, :].astype(jnp.float32)
            scaling = lax.rsqrt(jnp.mean(values * values, axis=-1, keepdims=True) + EPSILON)
            toks[seq, at, :] = (values * scaling * gain[...]).astype(jnp.bfloat16)

    mm_rows = rows // 2

    def make_bias():
        key = lax.broadcasted_iota(jnp.int32, (3 * WINDOW, WINDOW), 0)
        query = lax.broadcasted_iota(jnp.int32, (3 * WINDOW, WINDOW), 1)
        away = jnp.abs(query - key + WINDOW)
        for h in range(heads):
            slope = slopes[f * heads + h]
            bias[h] = jnp.where(away <= WINDOW, -slope * away.astype(jnp.float32), FAR)

    def project_qkv(seq):
        @pl.loop(0, 2)
        def _(b):
            at = pl.multiple_of(b * mm_rows, WINDOW)
            out = jnp.dot(
                toks[seq, pl.ds(at, mm_rows), :], wts[0], preferred_element_type=jnp.float32
            )
            qs[seq, pl.ds(at, mm_rows), :] = out[:, :qcols].astype(jnp.bfloat16)
            kvs[seq, pl.ds(at + WINDOW, mm_rows), :] = out[:, qcols:].astype(jnp.bfloat16)

    def edge_copies(buf, seq, width, sends, recvs, slot):
        length = buf.shape[1] if len(buf.shape) == 3 else buf.shape[2]
        ref = buf.at[seq] if len(buf.shape) == 3 else buf.at[slot // 2, seq]
        climb = pltpu.make_async_remote_copy(
            src_ref=ref.at[pl.ds(length - 2 * width, width)],
            dst_ref=ref.at[pl.ds(0, width)],
            send_sem=sends.at[slot, 0],
            recv_sem=recvs.at[slot, 0],
            device_id=up,
            device_id_type=MESH,
        )
        fall = pltpu.make_async_remote_copy(
            src_ref=ref.at[pl.ds(width, width)],
            dst_ref=ref.at[pl.ds(length - width, width)],
            send_sem=sends.at[slot, 1],
            recv_sem=recvs.at[slot, 1],
            device_id=down,
            device_id_type=MESH,
        )
        return ref, length, climb, fall

    def edges_start(buf, seq, width, sends, recvs, slot):
        ref, length, climb, fall = edge_copies(buf, seq, width, sends, recvs, slot)
        blank = jnp.zeros((width, ref.shape[1]), jnp.bfloat16)

        @pl.when(has_up)
        def _():
            climb.start()

        @pl.when(has_down)
        def _():
            fall.start()

        @pl.when(jnp.logical_not(has_up))
        def _():
            ref[pl.ds(length - width, width), :] = blank

        @pl.when(jnp.logical_not(has_down))
        def _():
            ref[pl.ds(0, width), :] = blank

    def edges_wait(buf, seq, width, sends, recvs, slot):
        _, _, climb, fall = edge_copies(buf, seq, width, sends, recvs, slot)

        @pl.when(has_up)
        def _():
            climb.wait_send()
            fall.wait_recv()

        @pl.when(has_down)
        def _():
            fall.wait_send()
            climb.wait_recv()

    def attend(seq, first, count):
        @pl.loop(first, first + count)
        def _(b):
            at = pl.multiple_of(b * WINDOW, WINDOW)
            kv = kvs[seq, pl.ds(at, 3 * WINDOW), :]
            keys = kv[:, :HEAD]
            values_t = kv.astype(jnp.float32).T[HEAD:, :].astype(jnp.bfloat16)
            queries = qs[seq, pl.ds(at, WINDOW), :]
            low = jnp.where((b == 0) & (s == 0), FAR, 0.0)
            high = jnp.where((b == blocks - 1) & (s == ns - 1), FAR, 0.0)
            outs = []
            for h in range(heads):
                query = queries[:, h * HEAD : (h + 1) * HEAD]
                scores = lax.dot_general(
                    keys, query, (((1,), (1,)), ((), ())), preferred_element_type=jnp.float32
                )
                scores = scores * (1.0 / math.sqrt(HEAD)) + bias[h]
                scores = jnp.concatenate(
                    [
                        scores[:WINDOW] + low,
                        scores[WINDOW : 2 * WINDOW],
                        scores[2 * WINDOW :] + high,
                    ],
                    axis=0,
                )
                sink = sinks[f * heads + h]
                peak = jnp.maximum(jnp.max(scores, axis=0, keepdims=True), sink)
                weights = jnp.exp(scores - peak)
                total = jnp.sum(weights, axis=0, keepdims=True) + jnp.exp(sink - peak)
                mixed = jnp.dot(
                    values_t, weights.astype(jnp.bfloat16), preferred_element_type=jnp.float32
                )
                outs.append(mixed / total)
                log_st[seq, pl.ds(h, 1), pl.ds(at, WINDOW)] = peak + jnp.log(total)
            stacked = jnp.concatenate(outs, axis=0)
            attn_st[seq, pl.ds(at, WINDOW), :] = stacked.T.astype(jnp.bfloat16)

    half_cols = pl.ds(pl.multiple_of(f * qcols, 128), qcols)

    def hand_back(src, dst, slot, seq_is_own):
        if seq_is_own:
            return pltpu.make_async_copy(src, dst, misc_sem.at[1 + slot])
        return pltpu.make_async_remote_copy(
            src_ref=src,
            dst_ref=dst,
            send_sem=ret_send.at[slot],
            recv_sem=ret_recv.at[slot],
            device_id=across,
            device_id_type=MESH,
        )

    def attn_return(own):
        seq = f if own else other
        return [
            hand_back(attn_st.at[seq], attn_out.at[:, half_cols], 0, own),
            hand_back(log_st.at[seq], log_out.at[f], 1, own),
        ]

    def conv_return(g, own):
        seq = f if own else other
        cols = pl.ds(pl.multiple_of(f * (2 * chans) + (g - 1) * chans, 128), chans)
        return [hand_back(conv_st.at[g - 1, seq], conv_out.at[:, cols], 1 + g, own)]

    def project_conv(g, seq):
        @pl.loop(0, 2)
        def _(b):
            at = pl.multiple_of(b * mm_rows, WINDOW)
            out = jnp.dot(
                toks[seq, pl.ds(at, mm_rows), :], wts[g], preferred_element_type=jnp.float32
            )
            inner = out[:, :chans].astype(jnp.bfloat16).astype(jnp.float32)
            signal = out[:, chans : 2 * chans].astype(jnp.bfloat16).astype(jnp.float32)
            prod[g - 1, seq, pl.ds(at + pad, mm_rows), :] = (inner * signal).astype(jnp.bfloat16)
            outer[seq, pl.ds(at, mm_rows), :] = out[:, 2 * chans :].astype(jnp.bfloat16)

    def mix(g, seq):
        cols = pl.ds(pl.multiple_of(f * (2 * chans) + (g - 1) * chans, 128), chans)
        tap = taps[:, cols]
        size = rows + 2 * pad
        full = prod[g - 1, seq].astype(jnp.float32)
        before = pltpu.roll(full, 1, 0)[pad : pad + rows]
        after = pltpu.roll(full, size - 1, 0)[pad : pad + rows]
        mixed = tap[0:1] * before + tap[1:2] * full[pad : pad + rows] + tap[2:3] * after
        conv_st[g - 1, seq] = (outer[seq].astype(jnp.float32) * mixed).astype(jnp.bfloat16)

    def begin(copies):
        for c in copies:
            c.start()

    def pass_tokens():
        return pltpu.make_async_remote_copy(
            src_ref=toks.at[other, share],
            dst_ref=toks.at[other, share],
            send_sem=tok_send.at[1],
            recv_sem=tok_recv.at[1],
            device_id=beside,
            device_id_type=MESH,
        )

    def take_tokens():
        tok_copy.wait_recv()
        pass_tokens().start()

    def ready_tokens():
        pass_tokens().wait_recv()
        pass_tokens().wait_send()
        norm_rows(other)

    def first_own():
        tok_load.wait()
        norm_rows(f)

    def kv_start(seq, slot):
        edges_start(kvs, seq, WINDOW, kv_send, kv_recv, slot)

    def kv_wait(seq, slot):
        edges_wait(kvs, seq, WINDOW, kv_send, kv_recv, slot)

    def pr_start(g, seq, slot):
        edges_start(prod, seq, pad, pr_send, pr_recv, (g - 1) * 2 + slot)

    def pr_wait(g, seq, slot):
        edges_wait(prod, seq, pad, pr_send, pr_recv, (g - 1) * 2 + slot)

    def qkv_own():
        project_qkv(f)
        kv_start(f, 0)

    def qkv_other():
        project_qkv(other)
        kv_start(other, 1)

    def finish_conv(g, own):
        seq, slot = (f, 0) if own else (other, 1)
        pr_wait(g, seq, slot)
        mix(g, seq)
        begin(conv_return(g, own))

    def both_parts(g, own):
        seq, slot = (f, 0) if own else (other, 1)
        project_conv(g, seq)
        pr_start(g, seq, slot)

    third = blocks // 3 if blocks % 3 == 0 else blocks
    parts = blocks // third

    def attend_part(seq, i):
        if i < parts:
            attend(seq, i * third, third)

    plan = {
        (0, 0): [make_bias],
        (0, 2): [first_own],
        (1, 0): [qkv_own],
        (1, 2): [lambda: kv_wait(f, 0), lambda: attend_part(f, 0)],
        (1, 3): [lambda: attend_part(f, 1)],
        (1, 4): [lambda: attend_part(f, 2), lambda: begin(attn_return(True))],
        (1, 7): [take_tokens],
        (2, 0): [lambda: both_parts(1, True)],
        (2, 1): [ready_tokens],
        (2, 2): [qkv_other, lambda: finish_conv(1, True)],
        (2, 3): [lambda: both_parts(1, False)],
        (2, 4): [lambda: kv_wait(other, 1), lambda: attend_part(other, 0)],
        (2, 5): [lambda: attend_part(other, 1)],
        (2, 6): [lambda: attend_part(other, 2), lambda: begin(attn_return(False))],
        (2, 7): [lambda: finish_conv(1, False)],
    }
    spare = dict(plan)
    for g in range(GROUPS):
        for d in range(ns):
            for par in range(2):
                relay_step(g, d, par)
                for piece in spare.pop((g, d * 2 + par), []):
                    piece()
        for key in sorted(k for k in spare if k[0] == g):
            for piece in spare.pop(key):
                piece()

    both_parts(2, False)
    finish_conv(2, False)
    both_parts(2, True)
    finish_conv(2, True)

    tok_copy.wait_send()
    settle()
    for own in (True, False):
        for c in attn_return(own) + conv_return(1, own) + conv_return(2, own):
            c.wait()


def fused_device(
    ns,
    tokens,
    norm_gain,
    query_weight,
    key_weight,
    value_weight,
    outer_weight,
    inner_weight,
    signal_weight,
    conv_taps,
    sink_logit,
):
    rows, width = tokens.shape[1:]
    depth, local = query_weight.shape
    qcols = local // 2
    heads = qcols // HEAD
    chans = outer_weight.shape[1] // 4
    head_local = 2 * heads
    head_index = lax.axis_index("tp") * head_local + jnp.arange(1, head_local + 1)
    slopes = jnp.exp2(-8.0 * head_index.astype(jnp.float32) / (head_local * lax.axis_size("tp")))
    kv_weight = jnp.stack(
        [
            jnp.concatenate([w[:, i * HEAD : (i + 1) * HEAD] for w in (key_weight, value_weight)], 1)
            for i in range(2)
        ]
    )
    group_cols = qcols + 2 * HEAD
    pad = 16
    bf, f32 = jnp.bfloat16, jnp.float32
    dma = pltpu.SemaphoreType.DMA
    hbm = pl.BlockSpec(memory_space=pl.ANY)
    vmem = pl.BlockSpec(memory_space=pltpu.VMEM)
    smem = pl.BlockSpec(memory_space=pltpu.SMEM)
    attended, conv, logs = pl.pallas_call(
        functools.partial(mega_kernel, ns),
        out_shape=(
            jax.ShapeDtypeStruct((rows, local), bf),
            jax.ShapeDtypeStruct((rows, 4 * chans), bf),
            jax.ShapeDtypeStruct((2, heads, rows), f32),
        ),
        in_specs=[hbm, vmem, hbm, hbm, hbm, hbm, hbm, vmem, smem, smem],
        out_specs=(hbm, hbm, hbm),
        scratch_shapes=[
            pltpu.VMEM((2, rows, width), bf),
            pltpu.VMEM((GROUPS, width, group_cols), bf),
            pltpu.VMEM((GROUPS, depth, group_cols), bf),
            pltpu.VMEM((2, rows, qcols), bf),
            pltpu.VMEM((2, rows + 2 * WINDOW, 2 * HEAD), bf),
            pltpu.VMEM((heads, 3 * WINDOW, WINDOW), f32),
            pltpu.VMEM((2, 2, rows + 2 * pad, chans), bf),
            pltpu.VMEM((2, rows, chans), bf),
            pltpu.VMEM((2, rows, qcols), bf),
            pltpu.VMEM((2, heads, rows), f32),
            pltpu.VMEM((2, 2, rows, chans), bf),
            dma((GROUPS, 3)),
            dma((GROUPS, 3)),
            dma((5,)),
            dma((GROUPS,)),
            dma((GROUPS, 2 * ns)),
            dma((GROUPS, 2 * ns)),
            dma((GROUPS, 2 * ns)),
            dma((2,)),
            dma((2,)),
            dma((2, 2)),
            dma((2, 2)),
            dma((4, 2)),
            dma((4, 2)),
            dma((4,)),
            dma((4,)),
        ],
        compiler_params=pltpu.CompilerParams(
            collective_id=0, has_side_effects=True, vmem_limit_bytes=48 << 20
        ),
    )(
        tokens[0],
        norm_gain[None],
        query_weight,
        kv_weight,
        outer_weight,
        inner_weight,
        signal_weight,
        conv_taps,
        slopes,
        sink_logit,
    )
    return (attended[None], conv[None], logs.reshape(1, head_local, rows))


def fits(mesh, args):
    tokens, query_weight, key_weight, outer_weight = (args[i] for i in (0, 2, 3, 5))
    sp, fs, tp = (mesh.shape[a] for a in ("sp", "fs", "tp"))
    rows = tokens.shape[1] // sp
    return (
        fs == 2
        and tokens.shape[0] == fs
        and tp % 2 == 0
        and rows % (2 * WINDOW) == 0
        and key_weight.shape[1] == 2 * HEAD * tp
        and query_weight.shape[1] % (256 * tp) == 0
        and outer_weight.shape[1] == 512 * tp
        and query_weight.shape[1] == 512 * tp
        and query_weight.shape[0] % (16 * sp * fs) == 0
    )


def solution(mesh):
    in_specs = (
        P("fs", "sp", None),
        P(),
        P(("sp", "fs"), "tp"),
        P(("sp", "fs"), "tp"),
        P(("sp", "fs"), "tp"),
        P(("sp", "fs"), "tp"),
        P(("sp", "fs"), "tp"),
        P(("sp", "fs"), "tp"),
        P(None, "tp"),
        P("tp"),
    )
    out_specs = (P("fs", "sp", "tp"), P("fs", "sp", "tp"), P("fs", "tp", "sp"))

    def run(*args):
        body = per_device
        if fits(mesh, args):
            body = functools.partial(fused_device, mesh.shape["sp"])
        return jax.shard_map(
            body, mesh=mesh, in_specs=in_specs, out_specs=out_specs, check_vma=False
        )(*args)

    return run
```

profile of v0, /device:TPU:0, one launch (start us, length us, event | category | flops | bytes accessed | tf_op | source)
XLA Modules:
  0.0 119.4 jit_solution(16885583508773986976)
XLA Ops:
  0.6 0.7 broadcast_in_dim.9.gain
  1.4 1.0 fusion
  2.4 1.0 fusion.1
  3.5 0.1 maximum_bitcast_fusion
  3.6 0.0 copy-start
  3.6 1.0 copy-done
  4.6 0.0 copy-start.1
  4.6 1.0 copy-done.1
  5.5 0.0 copy-start.2
  5.5 1.0 copy-done.2
  6.5 0.0 copy-start.3
  6.5 1.0 copy-done.3
  7.5 0.0 copy-start.4
  7.5 0.7 copy-done.4
  8.2 0.0 copy-start.5
  8.2 0.7 copy-done.5
  8.8 108.2 %shard_map.121 = (bf16[768,512]{1,0:T(8,128)(2,1)S(1)}, bf16[768,512]{1,0:T(8,128)(2,1)S(1)}, f32[2,4,768]{2,1,0:T(4,128)S(1)}) custom-call(bf16[768,2304]{1,0:T(8,128)(2,1)} %bitcast.9, f32[1,2304]{1,0:T(1,128)S(1)} %broadcast_in_dim.9.gain, bf16[288,512]{1,0:T(8,128)(2,1)S(1)} %copy-done, bf16[2,288,128]{2,1,0:T(8,128)(2,1)S(1)} %pad_maximum_fusion.kvw, ...), custom_call_target="tpu_custom_call" | custom-call | tf_op jit(solution)/shard_map/pallas_call | solution.py:678
  117.0 0.6 reshape.9
  117.6 0.9 copy.15
  118.5 0.9 copy.16
  (2 shorter events, 0.0 us)
Async XLA Ops:
  3.6 1.0 copy-start
  4.6 1.0 copy-start.1
  5.5 1.0 copy-start.2
  6.5 1.0 copy-start.3
  7.5 0.7 copy-start.4
  8.2 0.7 copy-start.5
where the time goes:
time: 120 us; the launch traced here: 119 us
  Pallas kernels  108 us (90%)
  local copies, waits for them, and re-layouts  10.4 us (9%)
    pallas_call x1, Pallas kernels, fused_device(): pl.pallas_call(functools.partial(mega_kernel, ns), out_shape=(jax.ShapeDt...  108 us
    unnamed x14, local copies, waits for them, and re-layouts  6.95 us

commit v1 on v0

--- a/solution.py
+++ b/solution.py
@@ -169,16 +169,17 @@
 
 def mega_kernel(
     ns,
+    tps,
     tokens,
-    gain,
+    gain_in,
     qw,
-    kvw,
+    kw,
+    vw,
     ow,
     iw,
     sw,
-    taps,
-    slopes,
-    sinks,
+    taps_in,
+    sinks_in,
     attn_out,
     conv_out,
     log_out,
@@ -193,6 +194,12 @@
     attn_st,
     log_st,
     conv_st,
+    kv_raw,
+    gain_raw,
+    gain,
+    taps,
+    sinks,
+    small_sem,
     load_sem,
     stage_sem,
     misc_sem,
@@ -243,10 +250,7 @@
     def loads(g, half, dest, sems):
         if g == 0:
             qc = pl.ds(pl.multiple_of(half * qcols, 128), qcols)
-            pairs = [
-                (qw.at[:, qc], dest.at[:, pl.ds(0, qcols)]),
-                (kvw.at[half], dest.at[:, pl.ds(qcols, 2 * HEAD)]),
-            ]
+            pairs = [(qw.at[:, qc], dest.at[:, pl.ds(0, qcols)])]
         else:
             c = pl.ds(pl.multiple_of(half * (2 * chans) + (g - 1) * chans, 128), chans)
             pairs = [
@@ -261,15 +265,36 @@
     theirs = s * 2 + other
     own_loads = [loads(g, f, wts.at[g, block_rows(mine)], load_sem) for g in range(GROUPS)]
     out_loads = [loads(g, other, stage_w.at[g], stage_sem) for g in range(GROUPS)]
+    small = [
+        pltpu.make_async_copy(a, b, small_sem.at[i])
+        for i, (a, b) in enumerate(
+            ((kw, kv_raw.at[0]), (vw, kv_raw.at[1]), (gain_in, gain_raw), (taps_in, taps), (sinks_in, sinks))
+        )
+    ]
+    small[0].start()
+    small[1].start()
     for g in range(GROUPS):
         for c in out_loads[g] + own_loads[g]:
             c.start()
+    for c in small[2:]:
+        c.start()
     tok_load = pltpu.make_async_copy(tokens, toks.at[f], misc_sem.at[0])
     tok_load.start()
 
     pl.semaphore_wait(
         barrier, 2 + jnp.where(has_up, 1, 0) + jnp.where(has_down, 1, 0)
     )
+
+    small[0].wait()
+    small[1].wait()
+    keys0, vals0 = kv_raw[0], kv_raw[1]
+    halves = [
+        jnp.concatenate([w[:, i * HEAD : (i + 1) * HEAD] for w in (keys0, vals0)], axis=1)
+        for i in range(2)
+    ]
+    first = f == 0
+    stage_w[0, :, pl.ds(qcols, 2 * HEAD)] = jnp.where(first, halves[1], halves[0])
+    wts[0, block_rows(mine), pl.ds(qcols, 2 * HEAD)] = jnp.where(first, halves[0], halves[1])
 
     y_copies = []
     for g in range(GROUPS):
@@ -380,11 +405,16 @@
     mm_rows = rows // 2
 
     def make_bias():
+        for c in small[2:]:
+            c.wait()
+        for i in range(gain_raw.shape[0]):
+            gain[:, i * 128 : (i + 1) * 128] = gain_raw[i : i + 1, :]
         key = lax.broadcasted_iota(jnp.int32, (3 * WINDOW, WINDOW), 0)
         query = lax.broadcasted_iota(jnp.int32, (3 * WINDOW, WINDOW), 1)
         away = jnp.abs(query - key + WINDOW)
         for h in range(heads):
-            slope = slopes[f * heads + h]
+            index = (t * (2 * heads) + f * heads + h + 1).astype(jnp.float32)
+            slope = jnp.exp2(jnp.full((1, WINDOW), -8.0 / (2 * heads * tps), jnp.float32) * index)
             bias[h] = jnp.where(away <= WINDOW, -slope * away.astype(jnp.float32), FAR)
 
     def project_qkv(seq):
@@ -643,6 +673,7 @@
 
 def fused_device(
     ns,
+    tps,
     tokens,
     norm_gain,
     query_weight,
@@ -660,30 +691,21 @@
     heads = qcols // HEAD
     chans = outer_weight.shape[1] // 4
     head_local = 2 * heads
-    head_index = lax.axis_index("tp") * head_local + jnp.arange(1, head_local + 1)
-    slopes = jnp.exp2(-8.0 * head_index.astype(jnp.float32) / (head_local * lax.axis_size("tp")))
-    kv_weight = jnp.stack(
-        [
-            jnp.concatenate([w[:, i * HEAD : (i + 1) * HEAD] for w in (key_weight, value_weight)], 1)
-            for i in range(2)
-        ]
-    )
     group_cols = qcols + 2 * HEAD
     pad = 16
     bf, f32 = jnp.bfloat16, jnp.float32
     dma = pltpu.SemaphoreType.DMA
-    hbm = pl.BlockSpec(memory_space=pl.ANY)
-    vmem = pl.BlockSpec(memory_space=pltpu.VMEM)
-    smem = pl.BlockSpec(memory_space=pltpu.SMEM)
+    hbm = pl.BlockSpec(memory_space=pltpu.HBM)
+    anyspace = pl.BlockSpec(memory_space=pl.ANY)
     attended, conv, logs = pl.pallas_call(
-        functools.partial(mega_kernel, ns),
+        functools.partial(mega_kernel, ns, tps),
         out_shape=(
             jax.ShapeDtypeStruct((rows, local), bf),
             jax.ShapeDtypeStruct((rows, 4 * chans), bf),
             jax.ShapeDtypeStruct((2, heads, rows), f32),
         ),
-        in_specs=[hbm, vmem, hbm, hbm, hbm, hbm, hbm, vmem, smem, smem],
-        out_specs=(hbm, hbm, hbm),
+        in_specs=[hbm] * 10,
+        out_specs=(anyspace, anyspace, anyspace),
         scratch_shapes=[
             pltpu.VMEM((2, rows, width), bf),
             pltpu.VMEM((GROUPS, width, group_cols), bf),
@@ -696,6 +718,12 @@
             pltpu.VMEM((2, rows, qcols), bf),
             pltpu.VMEM((2, heads, rows), f32),
             pltpu.VMEM((2, 2, rows, chans), bf),
+            pltpu.VMEM((2, depth, 2 * HEAD), bf),
+            pltpu.VMEM((width // 128, 128), f32),
+            pltpu.VMEM((1, width), f32),
+            pltpu.VMEM((3, 4 * chans), f32),
+            pltpu.SMEM((head_local,), f32),
+            dma((5,)),
             dma((GROUPS, 3)),
             dma((GROUPS, 3)),
             dma((5,)),
@@ -713,18 +741,18 @@
             dma((4,)),
         ],
         compiler_params=pltpu.CompilerParams(
-            collective_id=0, has_side_effects=True, vmem_limit_bytes=48 << 20
+            collective_id=0, has_side_effects=True, vmem_limit_bytes=67043328
         ),
     )(
         tokens[0],
-        norm_gain[None],
+        norm_gain.reshape(width // 128, 128),
         query_weight,
-        kv_weight,
+        key_weight,
+        value_weight,
         outer_weight,
         inner_weight,
         signal_weight,
         conv_taps,
-        slopes,
         sink_logit,
     )
     return (attended[None], conv[None], logs.reshape(1, head_local, rows))
@@ -765,7 +793,7 @@
     def run(*args):
         body = per_device
         if fits(mesh, args):
-            body = functools.partial(fused_device, mesh.shape["sp"])
+            body = functools.partial(fused_device, mesh.shape["sp"], mesh.shape["tp"])
         return jax.shard_map(
             body, mesh=mesh, in_specs=in_specs, out_specs=out_specs, check_vma=False
         )(*args)

time: 120 us -> 114 us (0.950)
  local copies, waits for them, and re-layouts: 10.4 us -> 5.48 us
    unnamed x14 -> x2, local copies, waits for them, and re-layouts: 6.95 us -> 4.12 us
    slice x2 -> x0, local copies, waits for them, and re-layouts: 2.09 us -> none  [fused_device(): w[:, i * HEAD:(i + 1) * HEAD]]
where the time goes in v1:
time: 114 us
  Pallas kernels  108 us (95%)
  local copies, waits for them, and re-layouts  5.48 us (5%)
    pallas_call x1, Pallas kernels, fused_device(): pl.pallas_call(functools.partial(mega_kernel, ns, tps), out_shape=(jax.Sh...  108 us
    unnamed x2, local copies, waits for them, and re-layouts  4.12 us

profile of v1, /device:TPU:0, one launch (start us, length us, event | category | flops | bytes accessed | tf_op | source)
XLA Modules:
  0.0 114.0 jit_solution(159128163800355801)
XLA Ops:
  0.6 107.9 %shard_map.121 = (bf16[768,512]{1,0:T(8,128)(2,1)}, bf16[768,512]{1,0:T(8,128)(2,1)}, f32[2,4,768]{2,1,0:T(4,128)}) custom-call(bf16[768,2304]{1,0:T(8,128)(2,1)} %bitcast.4, f32[18,128]{1,0:T(8,128)} %bitcast.7, bf16[288,512]{1,0:T(8,128)(2,1)} %qw.1, bf16[288,128]{1,0:T(8,128)(2,1)} %kw.1, bf16[288,128]{1,0:T(8,128)(2,1)} %vw.1, bf16[288,512]{1,0:T(8,128)(2,1)} %ow.1, ...), custom_call_target="tpu_custom_call" | custom-call | tf_op jit(solution)/shard_map/pallas_call | solution.py:700
  108.6 1.4 %reshape.13 = f32[1,8,768]{2,1,0:T(8,128)} reshape(f32[2,4,768]{2,1,0:T(4,128)} %get-tuple-element.8) | data formatting | bytes 49152 | tf_op jit(solution)/shard_map/reshape | solution.py:758
  109.9 2.1 %copy.15 = bf16[1,768,512]{2,1,0:T(8,128)(2,1)} copy(bf16[1,768,512]{2,1,0:T(8,128)(2,1)} %bitcast.6) | data formatting | bytes 1572864
  112.0 2.1 %copy.16 = bf16[1,768,512]{2,1,0:T(8,128)(2,1)} copy(bf16[1,768,512]{2,1,0:T(8,128)(2,1)} %bitcast.5) | data formatting | bytes 1572864

commit v2 on v1

v2 whole, which is shorter than its diff:
```python
import math

import functools

import jax
import jax.numpy as jnp
from jax import lax
from jax.experimental import pallas as pl
from jax.experimental.pallas import tpu as pltpu
from jax.sharding import PartitionSpec as P

HEAD = 64
WINDOW = 128


EPSILON = 1e-06


def extended(value, sides, width):
    for axis, dim in sides:
        size, length = (lax.axis_size(axis), value.shape[dim])
        up = [(i, (i + 1) % size) for i in range(size - 1)]
        down = [(j, i) for i, j in up]
        last = lax.slice_in_dim(value, length - width, length, axis=dim)
        initial = lax.slice_in_dim(value, 0, width, axis=dim)
        before = lax.ppermute(last, axis, up)
        after = lax.ppermute(initial, axis, down)
        value = jnp.concatenate([before, value, after], axis=dim)
    return value


def normalized(tokens, norm_gain):
    values = tokens.astype(jnp.float32)
    scaling = lax.rsqrt(jnp.mean(values * values, axis=-1, keepdims=True) + EPSILON)
    return (values * scaling * norm_gain).astype(jnp.bfloat16)


def folding(normed):

    def add_portions(running, portions, offset):
        return tuple(
            (jnp.dot(normed, portion, preferred_element_type=jnp.float32) for portion in portions)
        )

    return add_portions


def empty_sums(normed, weights):
    return tuple((jnp.zeros((normed.shape[0], weight.shape[1]), jnp.float32) for weight in weights))


def rounded(results):
    return tuple((result.astype(jnp.bfloat16) for result in results))


def gate_product(inner_gate, signal):
    return (inner_gate.astype(jnp.float32) * signal.astype(jnp.float32)).astype(jnp.bfloat16)


def send_edges(key_proj, value_proj, product):
    stacked = jnp.concatenate([key_proj, value_proj], axis=1)
    window_rows = extended(stacked, (("sp", 0),), WINDOW)
    conv_rows = extended(product, (("sp", 0),), 1)
    return (window_rows, conv_rows)


def banded_attention(queries, window_rows, sink_logit, slopes, first_pos, seq_length):
    tok_count = queries.shape[0]
    kv_cols = window_rows.shape[1] // 2
    kv_heads = kv_cols // HEAD
    group_size = queries.shape[1] // (HEAD * kv_heads)
    block_count = tok_count // WINDOW
    query_blocks = queries.reshape(block_count, WINDOW, kv_heads, group_size, HEAD)
    key_rows = window_rows[:, :kv_cols].reshape(block_count + 2, WINDOW, kv_heads, HEAD)
    value_rows = window_rows[:, kv_cols:].reshape(block_count + 2, WINDOW, kv_heads, HEAD)
    key_span = jnp.concatenate([key_rows[:-2], key_rows[1:-1], key_rows[2:]], axis=1)
    value_span = jnp.concatenate([value_rows[:-2], value_rows[1:-1], value_rows[2:]], axis=1)
    scores = jnp.einsum(
        "bqkgd,bskd->bkgqs", query_blocks, key_span, preferred_element_type=jnp.float32
    ) * (1.0 / math.sqrt(HEAD))
    distance = jnp.arange(WINDOW)[:, None] - jnp.arange(3 * WINDOW)[None, :] + WINDOW
    key_pos = (
        first_pos
        - WINDOW
        + WINDOW * jnp.arange(block_count)[:, None]
        + jnp.arange(3 * WINDOW)[None, :]
    )
    inside = (jnp.abs(distance)[None] <= WINDOW) & ((key_pos >= 0) & (key_pos < seq_length))[
        :, None, :
    ]
    scores = scores - slopes.reshape(kv_heads, group_size, 1, 1) * jnp.abs(distance).astype(
        jnp.float32
    )
    scores = jnp.where(inside[:, None, None], scores, -jnp.inf)
    sink_grid = sink_logit.reshape(kv_heads, group_size, 1, 1)
    row_peak = jnp.maximum(jnp.max(scores, axis=-1, keepdims=True), sink_grid)
    weights = jnp.exp(scores - row_peak)
    row_total = jnp.sum(weights, axis=-1, keepdims=True) + jnp.exp(sink_grid - row_peak)
    weighted = jnp.einsum(
        "bkgqs,bskd->bqkgd",
        weights.astype(jnp.bfloat16),
        value_span,
        preferred_element_type=jnp.float32,
    )
    attended = (
        (weighted / row_total.transpose(0, 3, 1, 2, 4))
        .astype(jnp.bfloat16)
        .reshape(tok_count, kv_heads * group_size * HEAD)
    )
    log_total = (
        (row_peak + jnp.log(row_total))[..., 0]
        .transpose(1, 2, 0, 3)
        .reshape(kv_heads * group_size, tok_count)
    )
    return (attended, log_total)


def per_device(
    tokens,
    norm_gain,
    query_weight,
    key_weight,
    value_weight,
    outer_weight,
    inner_weight,
    signal_weight,
    conv_taps,
    sink_logit,
):
    normed = normalized(tokens[0], norm_gain)
    add_portions = folding(normed)
    all_sums = add_portions(
        empty_sums(
            normed,
            (query_weight, key_weight, value_weight, outer_weight, inner_weight, signal_weight),
        ),
        (
            lax.all_gather(query_weight, ("sp", "fs"), axis=0, tiled=True),
            lax.all_gather(key_weight, ("sp", "fs"), axis=0, tiled=True),
            lax.all_gather(value_weight, ("sp", "fs"), axis=0, tiled=True),
            lax.all_gather(outer_weight, ("sp", "fs"), axis=0, tiled=True),
            lax.all_gather(inner_weight, ("sp", "fs"), axis=0, tiled=True),
            lax.all_gather(signal_weight, ("sp", "fs"), axis=0, tiled=True),
        ),
        jnp.int32(0),
    )
    queries, key_proj, value_proj, outer_gate, inner_gate, signal = rounded(all_sums)
    product = gate_product(inner_gate, signal)
    window_rows, conv_rows = send_edges(key_proj, value_proj, product)
    tok_count = normed.shape[0]
    head_local = queries.shape[1] // HEAD
    head_index = lax.axis_index("tp") * head_local + jnp.arange(1, head_local + 1)
    slopes = jnp.exp2(-8.0 * head_index.astype(jnp.float32) / (head_local * lax.axis_size("tp")))
    first_pos = lax.axis_index("sp") * tok_count
    attended, log_total = banded_attention(
        queries, window_rows, sink_logit, slopes, first_pos, tok_count * lax.axis_size("sp")
    )
    mixed_conv = conv_taps[0] * conv_rows[0:tok_count].astype(jnp.float32)
    mixed_conv = mixed_conv + conv_taps[1] * conv_rows[1 : tok_count + 1].astype(jnp.float32)
    mixed_conv = mixed_conv + conv_taps[2] * conv_rows[2 : tok_count + 2].astype(jnp.float32)
    conv_out = (outer_gate.astype(jnp.float32) * mixed_conv).astype(jnp.bfloat16)
    return (attended[None], conv_out[None], log_total[None])


MESH = pl.DeviceIdType.MESH
GROUPS = 3
SPAN = 4
SUBS = 4
FAR = -1e30


def mega_kernel(
    tps,
    tokens,
    gain_in,
    qw,
    kw,
    vw,
    ow,
    iw,
    sw,
    taps_in,
    sinks_in,
    attn_out,
    conv_out,
    log_out,
    toks,
    wts,
    stage_w,
    qs,
    kvs,
    bias,
    prod,
    outer,
    attn_st,
    log_st,
    conv_st,
    kv_raw,
    gain_raw,
    gain,
    taps,
    sinks,
    small_sem,
    load_sem,
    stage_sem,
    misc_sem,
    own_sem,
    y_send,
    w_recv,
    pair_send,
    mid_send,
    tok_y_send,
    tok_z_send,
    tok_t_send,
    tok_recv,
    kv_send,
    kv_recv,
    pr_send,
    pr_recv,
    ret_send,
    ret_recv,
    conv_send,
    conv_recv,
):
    s, f, t = lax.axis_index("sp"), lax.axis_index("fs"), lax.axis_index("tp")
    other = 1 - f
    core = lax.rem(t, 2)
    outward = 1 - lax.rem(s, 2)
    partner = s + 2 * outward - 1
    facing = SPAN - 1 - s
    far = SPAN - 1 - partner
    is_mid = (s == 1) | (s == SPAN - 2)
    is_end = jnp.logical_not(is_mid)
    low_half = s < SPAN // 2
    pair, diag, mid = (partner, f, t), (partner, other, t), (facing, f, t)
    across = (s, other, t)
    mate_t, beyond_t = t + 1 - 2 * core, lax.rem(t + 2, tps)
    mate, beyond = (s, f, mate_t), (s, f, beyond_t)
    rows = tokens.shape[0]
    depth = qw.shape[0]
    qcols = qs.shape[2]
    heads = qcols // HEAD
    chans = prod.shape[3]
    both_rows = outer.shape[2]
    blocks = rows // WINDOW
    pad = (prod.shape[2] - both_rows) // 2
    sub = rows // SUBS
    part = sub // tps
    up, down = (s + 1, f, t), (s - 1, f, t)
    has_up, has_down = s < SPAN - 1, s > 0
    own_off = jnp.where(low_half, rows, 0)
    end_off = rows - own_off

    barrier = pltpu.get_barrier_semaphore()
    for peer in (pair, diag, across, mate, beyond):
        pl.semaphore_signal(barrier, inc=1, device_id=peer, device_id_type=MESH)

    @pl.when(is_mid)
    def _():
        pl.semaphore_signal(barrier, inc=1, device_id=mid, device_id_type=MESH)

    def block_rows(blk):
        return pl.ds(pl.multiple_of(blk * depth, 16), depth)

    def loads(g, half, dest, sems):
        if g == 0:
            qc = pl.ds(pl.multiple_of(half * qcols, 128), qcols)
            pairs = [(qw.at[:, qc], dest.at[:, pl.ds(0, qcols)])]
        else:
            c = pl.ds(pl.multiple_of(half * (2 * chans) + (g - 1) * chans, 128), chans)
            pairs = [
                (ref.at[:, c], dest.at[:, pl.ds(i * chans, chans)])
                for i, ref in enumerate((iw, sw, ow))
            ]
        return [
            pltpu.make_async_copy(a, b, sems.at[g, i]) for i, (a, b) in enumerate(pairs)
        ]

    mine = s * 2 + f
    theirs = s * 2 + other
    own_loads = [loads(g, f, wts.at[g, block_rows(mine)], load_sem) for g in range(GROUPS)]
    out_loads = [loads(g, other, stage_w.at[g], stage_sem) for g in range(GROUPS)]
    small = [
        pltpu.make_async_copy(a, b, small_sem.at[i])
        for i, (a, b) in enumerate(
            (
                (kw, kv_raw.at[0]),
                (vw, kv_raw.at[1]),
                (gain_in, gain_raw),
                (taps_in, taps),
                (sinks_in, sinks),
            )
        )
    ]
    tok_load = pltpu.make_async_copy(tokens, toks.at[f], misc_sem.at[0])

    def begin(copies):
        for c in copies:
            c.start()

    def finish(copies):
        for c in copies:
            c.wait()

    begin(small[:2] + out_loads[0] + own_loads[0] + small[2:])
    tok_load.start()
    begin(out_loads[1] + own_loads[1] + out_loads[2] + own_loads[2])

    def remote(src, dst, send, recv, peer):
        return pltpu.make_async_remote_copy(
            src_ref=src,
            dst_ref=dst,
            send_sem=send,
            recv_sem=recv,
            device_id=peer,
            device_id_type=MESH,
        )

    def y_copy(g):
        return remote(
            stage_w.at[g], wts.at[g, block_rows(mine)], y_send.at[g], w_recv.at[g, mine], across
        )

    def block_copy(g, blk, sends, peer):
        at = wts.at[g, block_rows(blk)]
        return remote(at, at, sends.at[g, blk], w_recv.at[g, blk], peer)

    def to_pair(g, blk):
        return block_copy(g, blk, pair_send, pair)

    def to_mid(g, blk):
        return block_copy(g, blk, mid_send, mid)

    def arrived(g, blk):
        to_pair(g, blk).wait_recv()

    def slot_of(k):
        return (other, 2 + f, 2 + other)[k]

    def piece(slot, j, q):
        return toks.at[slot, pl.ds(pl.multiple_of(j * sub + q * part, 16), part)]

    def tok_y(k, j):
        slot = f if k == 0 else 2 + f
        at = piece(slot, j, t)
        return remote(at, at, tok_y_send.at[k, j], tok_recv.at[2 if k else 0, j, 0], across)

    def tok_z(k, j):
        seq = f if k == 0 else other
        return remote(
            piece(seq, j, t),
            piece(2 + seq, j, t),
            tok_z_send.at[k, j],
            tok_recv.at[1 + k, j, 0],
            pair,
        )

    def tok_share(k, j, kind):
        q = beyond_t if kind == 2 else t
        at = piece(slot_of(k), j, q)
        return remote(
            at, at, tok_t_send.at[k, j, kind], tok_recv.at[k, j, kind + 1],
            beyond if kind == 1 else mate,
        )

    def tok_wait(k, j, kind):
        at = piece(slot_of(k), j, t)
        remote(at, at, tok_t_send.at[k, j, 0], tok_recv.at[k, j, kind], mate).wait_recv()

    def take(k, j):
        tok_wait(k, j, 0)
        tok_share(k, j, 1).start()
        tok_share(k, j, 0).start()

    def hand(k, j):
        tok_wait(k, j, 2)
        tok_share(k, j, 2).start()

    def have(k, j):
        tok_wait(k, j, 1)
        tok_wait(k, j, 3)

    def norm_own():
        @pl.loop(0, blocks)
        def _(b):
            at = pl.ds(pl.multiple_of(b * WINDOW, WINDOW), WINDOW)
            values = toks[f, at, :].astype(jnp.float32)
            scaling = lax.rsqrt(jnp.mean(values * values, axis=-1, keepdims=True) + EPSILON)
            toks[f, at, :] = (values * scaling * gain[...]).astype(jnp.bfloat16)

    mm_rows = rows // 2

    def make_bias():
        key = lax.broadcasted_iota(jnp.int32, (3 * WINDOW, WINDOW), 0)
        query = lax.broadcasted_iota(jnp.int32, (3 * WINDOW, WINDOW), 1)
        away = jnp.abs(query - key + WINDOW)
        for h in range(heads):
            index = (t * (2 * heads) + f * heads + h + 1).astype(jnp.float32)
            slope = jnp.exp2(jnp.full((1, WINDOW), -8.0 / (2 * heads * tps), jnp.float32) * index)
            bias[h] = jnp.where(away <= WINDOW, -slope * away.astype(jnp.float32), FAR)

    def project_qkv(seq):
        @pl.loop(0, 2)
        def _(b):
            at = pl.multiple_of(b * mm_rows, WINDOW)
            out = jnp.dot(
                toks[seq, pl.ds(at, mm_rows), :], wts[0], preferred_element_type=jnp.float32
            )
            qs[seq, pl.ds(at, mm_rows), :] = out[:, :qcols].astype(jnp.bfloat16)
            kvs[seq, pl.ds(at + WINDOW, mm_rows), :] = out[:, qcols:].astype(jnp.bfloat16)

    kv_len = kvs.shape[1]

    def kv_copies(seq, slot):
        ref = kvs.at[seq]
        climb = remote(
            ref.at[pl.ds(kv_len - 2 * WINDOW, WINDOW)],
            ref.at[pl.ds(0, WINDOW)],
            kv_send.at[slot, 0],
            kv_recv.at[slot, 0],
            up,
        )
        fall = remote(
            ref.at[pl.ds(WINDOW, WINDOW)],
            ref.at[pl.ds(kv_len - WINDOW, WINDOW)],
            kv_send.at[slot, 1],
            kv_recv.at[slot, 1],
            down,
        )
        return climb, fall

    def kv_start(seq, slot):
        climb, fall = kv_copies(seq, slot)
        blank = jnp.zeros((WINDOW, 2 * HEAD), jnp.bfloat16)

        @pl.when(has_up)
        def _():
            climb.start()

        @pl.when(has_down)
        def _():
            fall.start()

        @pl.when(jnp.logical_not(has_up))
        def _():
            kvs[seq, pl.ds(kv_len - WINDOW, WINDOW), :] = blank

        @pl.when(jnp.logical_not(has_down))
        def _():
            kvs[seq, pl.ds(0, WINDOW), :] = blank

    def kv_wait(seq, slot):
        climb, fall = kv_copies(seq, slot)

        @pl.when(has_up)
        def _():
            climb.wait_send()
            fall.wait_recv()

        @pl.when(has_down)
        def _():
            fall.wait_send()
            climb.wait_recv()

    def attend(seq, first, count, step=1):
        @pl.loop(0, count)
        def _(i):
            b = first + i * step
            at = pl.multiple_of(b * WINDOW, WINDOW)
            kv = kvs[seq, pl.ds(at, 3 * WINDOW), :]
            keys = kv[:, :HEAD]
            values_t = kv.astype(jnp.float32).T[HEAD:, :].astype(jnp.bfloat16)
            queries = qs[seq, pl.ds(at, WINDOW), :]
            low = jnp.where((b == 0) & (s == 0), FAR, 0.0)
            high = jnp.where((b == blocks - 1) & (s == SPAN - 1), FAR, 0.0)
            outs = []
            for h in range(heads):
                query = queries[:, h * HEAD : (h + 1) * HEAD]
                scores = lax.dot_general(
                    keys, query, (((1,), (1,)), ((), ())), preferred_element_type=jnp.float32
                )
                scores = scores * (1.0 / math.sqrt(HEAD)) + bias[h]
                scores = jnp.concatenate(
                    [
                        scores[:WINDOW] + low,
                        scores[WINDOW : 2 * WINDOW],
                        scores[2 * WINDOW :] + high,
                    ],
                    axis=0,
                )
                sink = sinks[f * heads + h]
                peak = jnp.maximum(jnp.max(scores, axis=0, keepdims=True), sink)
                weights = jnp.exp(scores - peak)
                total = jnp.sum(weights, axis=0, keepdims=True) + jnp.exp(sink - peak)
                mixed = jnp.dot(
                    values_t, weights.astype(jnp.bfloat16), preferred_element_type=jnp.float32
                )
                outs.append(mixed / total)
                log_st[seq, pl.ds(h, 1), pl.ds(at, WINDOW)] = peak + jnp.log(total)
            stacked = jnp.concatenate(outs, axis=0)
            attn_st[seq, pl.ds(at, WINDOW), :] = stacked.T.astype(jnp.bfloat16)

    half_cols = pl.ds(pl.multiple_of(f * qcols, 128), qcols)

    def attn_return(own):
        seq = f if own else other
        pairs = [
            (attn_st.at[seq], attn_out.at[:, half_cols]),
            (log_st.at[seq], log_out.at[f]),
        ]
        if own:
            return [pltpu.make_async_copy(a, b, misc_sem.at[1 + i]) for i, (a, b) in enumerate(pairs)]
        return [
            remote(a, b, ret_send.at[i], ret_recv.at[i], across) for i, (a, b) in enumerate(pairs)
        ]

    def conv_cols(g):
        return pl.ds(pl.multiple_of(f * (2 * chans) + (g - 1) * chans, 128), chans)

    def conv_return(g, own_seq, own_rows):
        seq = f if own_seq else other
        off = own_off if own_rows else end_off
        src = conv_st.at[g - 1, seq, pl.ds(pl.multiple_of(off, WINDOW), rows)]
        dst = conv_out.at[:, conv_cols(g)]
        if own_seq and own_rows:
            return pltpu.make_async_copy(src, dst, own_sem.at[g - 1])
        which = 0 if own_seq else 1
        kind = 0 if own_seq else (2 if own_rows else 1)
        peer = pair if own_seq else (across if own_rows else diag)
        return remote(src, dst, conv_send.at[g - 1, kind], conv_recv.at[g - 1, which], peer)

    def project_conv(g, seq, own_rows):
        slot, off = (seq, own_off) if own_rows else (2 + seq, end_off)

        @pl.loop(0, 2)
        def _(b):
            at = pl.multiple_of(b * mm_rows, WINDOW)
            to = pl.multiple_of(off + b * mm_rows, WINDOW)
            out = jnp.dot(
                toks[slot, pl.ds(at, mm_rows), :], wts[g], preferred_element_type=jnp.float32
            )
            inner = out[:, :chans].astype(jnp.bfloat16).astype(jnp.float32)
            signal = out[:, chans : 2 * chans].astype(jnp.bfloat16).astype(jnp.float32)
            prod[g - 1, seq, pl.ds(to + pad, mm_rows), :] = (inner * signal).astype(jnp.bfloat16)
            outer[g - 1, seq, pl.ds(to, mm_rows), :] = out[:, 2 * chans :].astype(jnp.bfloat16)

    def pr_copies(g, seq, slot):
        ref = prod.at[g - 1, seq]
        climb = remote(
            ref.at[pl.ds(both_rows, pad)],
            ref.at[pl.ds(0, pad)],
            pr_send.at[g - 1, slot],
            pr_recv.at[g - 1, slot],
            mid,
        )
        fall = remote(
            ref.at[pl.ds(pad, pad)],
            ref.at[pl.ds(both_rows + pad, pad)],
            pr_send.at[g - 1, slot],
            pr_recv.at[g - 1, slot],
            mid,
        )
        return climb, fall

    def pr_start(g, seq, slot):
        climb, fall = pr_copies(g, seq, slot)
        blank = jnp.zeros((pad, chans), jnp.bfloat16)

        @pl.when(low_half)
        def _():
            climb.start()
            prod[g - 1, seq, pl.ds(0, pad), :] = blank

        @pl.when(jnp.logical_not(low_half))
        def _():
            fall.start()
            prod[g - 1, seq, pl.ds(both_rows + pad, pad), :] = blank

    def pr_wait(g, seq, slot):
        climb, fall = pr_copies(g, seq, slot)

        @pl.when(low_half)
        def _():
            climb.wait_send()
            fall.wait_recv()

        @pl.when(jnp.logical_not(low_half))
        def _():
            fall.wait_send()
            climb.wait_recv()

    def mix(g, seq, own_rows):
        off = pl.multiple_of(own_off if own_rows else end_off, WINDOW)
        tap = taps[:, conv_cols(g)]
        size = rows + 2 * pad
        full = prod[g - 1, seq, pl.ds(off, size), :].astype(jnp.float32)
        before = pltpu.roll(full, 1, 0)[pad : pad + rows]
        after = pltpu.roll(full, size - 1, 0)[pad : pad + rows]
        mixed = tap[0:1] * before + tap[1:2] * full[pad : pad + rows] + tap[2:3] * after
        gate = outer[g - 1, seq, pl.ds(off, rows), :].astype(jnp.float32)
        conv_st[g - 1, seq, pl.ds(off, rows), :] = (gate * mixed).astype(jnp.bfloat16)

    finish(small[:2])
    keys0, vals0 = kv_raw[0], kv_raw[1]
    halves = [
        jnp.concatenate([w[:, i * HEAD : (i + 1) * HEAD] for w in (keys0, vals0)], axis=1)
        for i in range(2)
    ]
    first = f == 0
    stage_w[0, :, pl.ds(qcols, 2 * HEAD)] = jnp.where(first, halves[1], halves[0])
    wts[0, block_rows(mine), pl.ds(qcols, 2 * HEAD)] = jnp.where(first, halves[0], halves[1])

    pl.semaphore_wait(barrier, jnp.where(is_mid, 6, 5))

    finish(own_loads[0])
    to_pair(0, mine).start()

    @pl.when(is_mid)
    def _():
        to_mid(0, mine).start()

    finish(out_loads[0])
    y_copy(0).start()
    finish(out_loads[1])
    y_copy(1).start()
    finish(own_loads[1])

    @pl.when(is_mid)
    def _():
        to_mid(1, mine).start()

    finish(small[2:])
    for i in range(gain_raw.shape[0]):
        gain[:, i * 128 : (i + 1) * 128] = gain_raw[i : i + 1, :]
    tok_load.wait()
    norm_own()
    for j in range(SUBS // 2):
        tok_y(0, j).start()
    finish(out_loads[2] + own_loads[2])
    y_copy(2).start()
    for j in range(SUBS // 2, SUBS):
        tok_y(0, j).start()

    def relay(g, blk, onward):
        arrived(g, blk)
        onward(g, blk).start()

    pt = [partner * 2 + f, partner * 2 + other]
    ct = [facing * 2 + f, facing * 2 + other]
    ft = [far * 2 + f, far * 2 + other]

    def end_program():
        tok_z(0, 0).start()
        relay(0, theirs, to_pair)
        tok_z(0, 1).start()
        to_pair(1, mine).start()
        relay(1, theirs, to_pair)
        tok_z(0, 2).start()
        tok_z(0, 3).start()
        to_pair(2, mine).start()
        make_bias()
        take(0, 0)
        take(0, 1)
        hand(0, 0)
        relay(2, theirs, to_pair)
        hand(0, 1)
        take(0, 2)
        tok_z(1, 2).start()
        hand(0, 2)
        take(0, 3)
        tok_z(1, 3).start()
        for blk in pt + ct + ft:
            arrived(0, blk)
        project_qkv(f)
        kv_start(f, 0)
        hand(0, 3)
        for j in range(SUBS):
            have(0, j)
        project_qkv(other)
        kv_start(other, 1)
        attend(f, 1, blocks - 2)
        kv_wait(f, 0)
        attend(f, 0, 2, blocks - 1)
        begin(attn_return(True))
        attend(other, 1, blocks - 2)
        kv_wait(other, 1)
        attend(other, 0, 2, blocks - 1)
        begin(attn_return(False))
        for g in (1, 2):
            for own_seq in (True, False):
                conv_return(g, own_seq, False).wait_recv()
        for g in range(GROUPS):
            to_pair(g, mine).wait_send()
            to_pair(g, theirs).wait_send()
        for j in range(SUBS):
            tok_z(0, j).wait_send()
        for j in range(SUBS // 2, SUBS):
            tok_z(1, j).wait_send()

    def conv_own(g, own_seq):
        seq, slot = (f, 0) if own_seq else (other, 1)
        project_conv(g, seq, True)
        pr_start(g, seq, slot)

    def conv_end(g, own_seq):
        seq = f if own_seq else other
        project_conv(g, seq, False)
        mix(g, seq, False)
        conv_return(g, own_seq, False).start()

    def conv_close(g, own_seq):
        seq, slot = (f, 0) if own_seq else (other, 1)
        pr_wait(g, seq, slot)
        mix(g, seq, True)
        conv_return(g, own_seq, True).start()

    def mid_program():
        make_bias()
        relay(0, theirs, to_mid)
        to_pair(0, theirs).start()
        relay(1, theirs, to_mid)
        relay(0, ct[0], to_pair)
        relay(0, pt[0], to_mid)
        take(1, 0)
        tok_y(1, 0).start()
        take(0, 0)
        relay(0, pt[1], to_mid)
        to_mid(2, mine).start()
        relay(0, ct[1], to_pair)
        hand(1, 0)
        take(1, 1)
        tok_y(1, 1).start()
        take(0, 1)
        hand(0, 0)
        relay(2, theirs, to_mid)
        relay(1, pt[0], to_mid)
        hand(1, 1)
        relay(0, ft[0], to_pair)
        take(2, 0)
        hand(0, 1)
        relay(1, pt[1], to_mid)
        relay(0, ft[1], to_pair)
        project_qkv(f)
        kv_start(f, 0)
        take(0, 2)
        take(2, 1)
        hand(2, 0)
        attend(f, 1, (blocks - 2) // 2)
        take(0, 3)
        take(1, 2)
        hand(0, 2)
        hand(2, 1)
        attend(f, 1 + (blocks - 2) // 2, (blocks - 2) // 2)
        take(1, 3)
        hand(0, 3)
        hand(1, 2)
        for j in range(SUBS):
            have(0, j)
        project_qkv(other)
        kv_start(other, 1)
        relay(2, pt[0], to_mid)
        hand(1, 3)
        kv_wait(f, 0)
        attend(f, 0, 2, blocks - 1)
        begin(attn_return(True))
        relay(2, pt[1], to_mid)
        attend(other, 1, blocks - 2)
        kv_wait(other, 1)
        attend(other, 0, 2, blocks - 1)
        begin(attn_return(False))
        for blk in ct + ft:
            arrived(1, blk)
        conv_own(1, True)
        conv_own(1, False)
        take(2, 2)
        for j in range(SUBS):
            have(1, j)
        conv_end(1, True)
        hand(2, 2)
        take(2, 3)
        conv_close(1, True)
        hand(2, 3)
        for blk in ct + ft:
            arrived(2, blk)
        conv_own(2, True)
        conv_own(2, False)
        conv_end(2, True)
        conv_close(2, True)
        for j in range(SUBS):
            have(2, j)
        conv_end(1, False)
        conv_end(2, False)
        conv_close(1, False)
        conv_close(2, False)
        for g in (1, 2):
            conv_return(g, False, True).wait_recv()
            conv_return(g, True, True).wait()
            conv_return(g, False, True).wait_send()
            for own_seq in (True, False):
                conv_return(g, own_seq, False).wait_send()
        for blk in [mine, theirs] + ct + ft:
            to_pair(0, blk).wait_send()
        for g in range(GROUPS):
            for blk in [mine, theirs] + pt:
                to_mid(g, blk).wait_send()
        for j in range(SUBS // 2):
            tok_y(1, j).wait_send()
        for k in (1, 2):
            for j in range(SUBS):
                for kind in range(3):
                    tok_share(k, j, kind).wait_send()

    pl.when(is_end)(end_program)
    pl.when(is_mid)(mid_program)

    for g in range(GROUPS):
        y_copy(g).wait_send()
    for j in range(SUBS):
        tok_y(0, j).wait_send()
        for kind in range(3):
            tok_share(0, j, kind).wait_send()
    for own in (True, False):
        finish(attn_return(own))


def fused_device(
    tps,
    tokens,
    norm_gain,
    query_weight,
    key_weight,
    value_weight,
    outer_weight,
    inner_weight,
    signal_weight,
    conv_taps,
    sink_logit,
):
    rows, width = tokens.shape[1:]
    depth, local = query_weight.shape
    qcols = local // 2
    heads = qcols // HEAD
    chans = outer_weight.shape[1] // 4
    head_local = 2 * heads
    group_cols = qcols + 2 * HEAD
    pad = 16
    bf, f32 = jnp.bfloat16, jnp.float32
    dma = pltpu.SemaphoreType.DMA
    hbm = pl.BlockSpec(memory_space=pltpu.HBM)
    anyspace = pl.BlockSpec(memory_space=pl.ANY)
    attended, conv, logs = pl.pallas_call(
        functools.partial(mega_kernel, tps),
        out_shape=(
            jax.ShapeDtypeStruct((rows, local), bf),
            jax.ShapeDtypeStruct((rows, 4 * chans), bf),
            jax.ShapeDtypeStruct((2, heads, rows), f32),
        ),
        in_specs=[hbm] * 10,
        out_specs=(anyspace, anyspace, anyspace),
        scratch_shapes=[
            pltpu.VMEM((4, rows, width), bf),
            pltpu.VMEM((GROUPS, width, group_cols), bf),
            pltpu.VMEM((GROUPS, depth, group_cols), bf),
            pltpu.VMEM((2, rows, qcols), bf),
            pltpu.VMEM((2, rows + 2 * WINDOW, 2 * HEAD), bf),
            pltpu.VMEM((heads, 3 * WINDOW, WINDOW), f32),
            pltpu.VMEM((2, 2, 2 * rows + 2 * pad, chans), bf),
            pltpu.VMEM((2, 2, 2 * rows, chans), bf),
            pltpu.VMEM((2, rows, qcols), bf),
            pltpu.VMEM((2, heads, rows), f32),
            pltpu.VMEM((2, 2, 2 * rows, chans), bf),
            pltpu.VMEM((2, depth, 2 * HEAD), bf),
            pltpu.VMEM((width // 128, 128), f32),
            pltpu.VMEM((1, width), f32),
            pltpu.VMEM((3, 4 * chans), f32),
            pltpu.SMEM((head_local,), f32),
            dma((5,)),
            dma((GROUPS, 3)),
            dma((GROUPS, 3)),
            dma((3,)),
            dma((2,)),
            dma((GROUPS,)),
            dma((GROUPS, 2 * SPAN)),
            dma((GROUPS, 2 * SPAN)),
            dma((GROUPS, 2 * SPAN)),
            dma((2, SUBS)),
            dma((2, SUBS)),
            dma((3, SUBS, 3)),
            dma((3, SUBS, 4)),
            dma((2, 2)),
            dma((2, 2)),
            dma((2, 2)),
            dma((2, 2)),
            dma((2,)),
            dma((2,)),
            dma((2, 3)),
            dma((2, 2)),
        ],
        compiler_params=pltpu.CompilerParams(
            collective_id=0, has_side_effects=True, vmem_limit_bytes=67043328
        ),
    )(
        tokens[0],
        norm_gain.reshape(width // 128, 128),
        query_weight,
        key_weight,
        value_weight,
        outer_weight,
        inner_weight,
        signal_weight,
        conv_taps,
        sink_logit,
    )
    return (attended[None], conv[None], logs.reshape(1, head_local, rows))


def fits(mesh, args):
    tokens, query_weight, key_weight, outer_weight = (args[i] for i in (0, 2, 3, 5))
    sp, fs, tp = (mesh.shape[a] for a in ("sp", "fs", "tp"))
    rows = tokens.shape[1] // sp
    return (
        fs == 2
        and sp == SPAN
        and tokens.shape[0] == fs
        and tp == 4
        and rows % (2 * WINDOW) == 0
        and rows // WINDOW % 2 == 0
        and rows % (16 * SUBS * tp) == 0
        and key_weight.shape[1] == 2 * HEAD * tp
        and query_weight.shape[1] % (256 * tp) == 0
        and outer_weight.shape[1] == 512 * tp
        and query_weight.shape[1] == 512 * tp
        and query_weight.shape[0] % (16 * sp * fs) == 0
    )


def solution(mesh):
    in_specs = (
        P("fs", "sp", None),
        P(),
        P(("sp", "fs"), "tp"),
        P(("sp", "fs"), "tp"),
        P(("sp", "fs"), "tp"),
        P(("sp", "fs"), "tp"),
        P(("sp", "fs"), "tp"),
        P(("sp", "fs"), "tp"),
        P(None, "tp"),
        P("tp"),
    )
    out_specs = (P("fs", "sp", "tp"), P("fs", "sp", "tp"), P("fs", "tp", "sp"))

    def run(*args):
        body = per_device
        if fits(mesh, args):
            body = functools.partial(fused_device, mesh.shape["tp"])
        return jax.shard_map(
            body, mesh=mesh, in_specs=in_specs, out_specs=out_specs, check_vma=False
        )(*args)

    return run
```

time: 114 us -> 124 us (1.088)
  Pallas kernels: 108 us -> 117 us
    pallas_call x1, Pallas kernels: 108 us -> 117 us  [fused_device(): pl.pallas_call(functools.partial(mega_kernel, tps), out_shape=(jax.ShapeD...]
where the time goes in v2:
time: 124 us; the launch traced here: 123 us
  Pallas kernels  117 us (94%)
  local copies, waits for them, and re-layouts  5.48 us (4%)
    pallas_call x1, Pallas kernels, fused_device(): pl.pallas_call(functools.partial(mega_kernel, tps), out_shape=(jax.ShapeD...  117 us
    unnamed x2, local copies, waits for them, and re-layouts  4.12 us

profile of v2, /device:TPU:0, one launch (start us, length us, event | category | flops | bytes accessed | tf_op | source)
XLA Modules:
  0.0 123.2 jit_solution(947428758863665366)
XLA Ops:
  0.6 117.1 %shard_map.121 = (bf16[768,512]{1,0:T(8,128)(2,1)}, bf16[768,512]{1,0:T(8,128)(2,1)}, f32[2,4,768]{2,1,0:T(4,128)}) custom-call(bf16[768,2304]{1,0:T(8,128)(2,1)} %bitcast.4, f32[18,128]{1,0:T(8,128)} %bitcast.7, bf16[288,512]{1,0:T(8,128)(2,1)} %qw.1, bf16[288,128]{1,0:T(8,128)(2,1)} %kw.1, bf16[288,128]{1,0:T(8,128)(2,1)} %vw.1, bf16[288,512]{1,0:T(8,128)(2,1)} %ow.1, ...), custom_call_target="tpu_custom_call" | custom-call | tf_op jit(solution)/shard_map/pallas_call | solution.py:851
  117.8 1.4 %reshape.13 = f32[1,8,768]{2,1,0:T(8,128)} reshape(f32[2,4,768]{2,1,0:T(4,128)} %get-tuple-element.8) | data formatting | bytes 49152 | tf_op jit(solution)/shard_map/reshape | solution.py:914
  119.1 2.1 %copy.15 = bf16[1,768,512]{2,1,0:T(8,128)(2,1)} copy(bf16[1,768,512]{2,1,0:T(8,128)(2,1)} %bitcast.6) | data formatting | bytes 1572864
  121.2 2.1 %copy.16 = bf16[1,768,512]{2,1,0:T(8,128)(2,1)} copy(bf16[1,768,512]{2,1,0:T(8,128)(2,1)} %bitcast.5) | data formatting | bytes 1572864

commit v3 on v2

--- a/solution.py
+++ b/solution.py
@@ -195,6 +195,7 @@
     attn_st,
     log_st,
     conv_st,
+    acc,
     kv_raw,
     gain_raw,
     gain,
@@ -342,8 +343,9 @@
 
     def tok_y(k, j):
         slot = f if k == 0 else 2 + f
-        at = piece(slot, j, t)
-        return remote(at, at, tok_y_send.at[k, j], tok_recv.at[2 if k else 0, j, 0], across)
+        at = piece(slot, j, beyond_t if k == 2 else t)
+        kind = 2 if k == 2 else 0
+        return remote(at, at, tok_y_send.at[k, j], tok_recv.at[2 if k else 0, j, kind], across)
 
     def tok_z(k, j):
         seq = f if k == 0 else other
@@ -369,12 +371,17 @@
 
     def take(k, j):
         tok_wait(k, j, 0)
-        tok_share(k, j, 1).start()
+        if k < 2 or j >= SUBS // 2:
+            tok_share(k, j, 1).start()
         tok_share(k, j, 0).start()
+        if k == 1 and j < SUBS // 2:
+            tok_y(1, j).start()
 
     def hand(k, j):
         tok_wait(k, j, 2)
         tok_share(k, j, 2).start()
+        if k == 1 and j < SUBS // 2:
+            tok_y(2, j).start()
 
     def have(k, j):
         tok_wait(k, j, 1)
@@ -399,13 +406,34 @@
             slope = jnp.exp2(jnp.full((1, WINDOW), -8.0 / (2 * heads * tps), jnp.float32) * index)
             bias[h] = jnp.where(away <= WINDOW, -slope * away.astype(jnp.float32), FAR)
 
+    half_k = depth * SPAN
+    near_k = pl.multiple_of(jnp.where(low_half, 0, half_k), 128)
+    far_k = pl.multiple_of(half_k - near_k, 128)
+
+    def partial(g, slot, at, k_off):
+        return jnp.dot(
+            toks[slot, pl.ds(at, mm_rows), pl.ds(k_off, half_k)],
+            wts[g, pl.ds(k_off, half_k), :],
+            preferred_element_type=jnp.float32,
+        )
+
+    def sums(g, slot):
+        return slot if g == 0 else slot + 4 * g - 2
+
+    def near(g, slot, lo=0, hi=2):
+        @pl.loop(lo, hi)
+        def _(b):
+            at = pl.multiple_of(b * mm_rows, WINDOW)
+            acc[sums(g, slot), pl.ds(at, mm_rows), :] = partial(g, slot, at, near_k)
+
+    def total(g, slot, at):
+        return acc[sums(g, slot), pl.ds(at, mm_rows), :] + partial(g, slot, at, far_k)
+
     def project_qkv(seq):
         @pl.loop(0, 2)
         def _(b):
             at = pl.multiple_of(b * mm_rows, WINDOW)
-            out = jnp.dot(
-                toks[seq, pl.ds(at, mm_rows), :], wts[0], preferred_element_type=jnp.float32
-            )
+            out = total(0, seq, at)
             qs[seq, pl.ds(at, mm_rows), :] = out[:, :qcols].astype(jnp.bfloat16)
             kvs[seq, pl.ds(at + WINDOW, mm_rows), :] = out[:, qcols:].astype(jnp.bfloat16)
 
@@ -517,28 +545,34 @@
     def conv_cols(g):
         return pl.ds(pl.multiple_of(f * (2 * chans) + (g - 1) * chans, 128), chans)
 
-    def conv_return(g, own_seq, own_rows):
+    split = mm_rows - pad
+
+    def conv_return(g, own_seq, own_rows, tail=0):
         seq = f if own_seq else other
         off = own_off if own_rows else end_off
-        src = conv_st.at[g - 1, seq, pl.ds(pl.multiple_of(off, WINDOW), rows)]
-        dst = conv_out.at[:, conv_cols(g)]
+        lo, count = 0, rows
+        if not own_seq and not own_rows:
+            lo, count = (split, rows - split) if tail else (0, split)
+        src = conv_st.at[g - 1, seq, pl.ds(pl.multiple_of(off + lo, pad), count)]
+        dst = conv_out.at[pl.ds(lo, count), conv_cols(g)]
         if own_seq and own_rows:
             return pltpu.make_async_copy(src, dst, own_sem.at[g - 1])
-        which = 0 if own_seq else 1
-        kind = 0 if own_seq else (2 if own_rows else 1)
-        peer = pair if own_seq else (across if own_rows else diag)
-        return remote(src, dst, conv_send.at[g - 1, kind], conv_recv.at[g - 1, which], peer)
-
-    def project_conv(g, seq, own_rows):
+        if own_seq:
+            return remote(src, dst, conv_send.at[g - 1, 0], conv_recv.at[g - 1, 0], pair)
+        if own_rows:
+            return remote(src, dst, conv_send.at[g - 1, 1], conv_recv.at[g - 1, 1], across)
+        return remote(
+            src, dst, conv_send.at[g - 1, 2 + tail], conv_recv.at[g - 1, 1 + tail], diag
+        )
+
+    def project_conv(g, seq, own_rows, lo=0, hi=2):
         slot, off = (seq, own_off) if own_rows else (2 + seq, end_off)
 
-        @pl.loop(0, 2)
+        @pl.loop(lo, hi)
         def _(b):
             at = pl.multiple_of(b * mm_rows, WINDOW)
             to = pl.multiple_of(off + b * mm_rows, WINDOW)
-            out = jnp.dot(
-                toks[slot, pl.ds(at, mm_rows), :], wts[g], preferred_element_type=jnp.float32
-            )
+            out = total(g, slot, at)
             inner = out[:, :chans].astype(jnp.bfloat16).astype(jnp.float32)
             signal = out[:, chans : 2 * chans].astype(jnp.bfloat16).astype(jnp.float32)
             prod[g - 1, seq, pl.ds(to + pad, mm_rows), :] = (inner * signal).astype(jnp.bfloat16)
@@ -589,16 +623,17 @@
             fall.wait_send()
             climb.wait_recv()
 
-    def mix(g, seq, own_rows):
-        off = pl.multiple_of(own_off if own_rows else end_off, WINDOW)
+    def mix(g, seq, own_rows, lo=0, hi=None):
+        count = (rows if hi is None else hi) - lo
+        off = pl.multiple_of((own_off if own_rows else end_off) + lo, pad)
         tap = taps[:, conv_cols(g)]
-        size = rows + 2 * pad
+        size = count + 2 * pad
         full = prod[g - 1, seq, pl.ds(off, size), :].astype(jnp.float32)
-        before = pltpu.roll(full, 1, 0)[pad : pad + rows]
-        after = pltpu.roll(full, size - 1, 0)[pad : pad + rows]
-        mixed = tap[0:1] * before + tap[1:2] * full[pad : pad + rows] + tap[2:3] * after
-        gate = outer[g - 1, seq, pl.ds(off, rows), :].astype(jnp.float32)
-        conv_st[g - 1, seq, pl.ds(off, rows), :] = (gate * mixed).astype(jnp.bfloat16)
+        before = pltpu.roll(full, 1, 0)[pad : pad + count]
+        after = pltpu.roll(full, size - 1, 0)[pad : pad + count]
+        mixed = tap[0:1] * before + tap[1:2] * full[pad : pad + count] + tap[2:3] * after
+        gate = outer[g - 1, seq, pl.ds(off, count), :].astype(jnp.float32)
+        conv_st[g - 1, seq, pl.ds(off, count), :] = (gate * mixed).astype(jnp.bfloat16)
 
     finish(small[:2])
     keys0, vals0 = kv_raw[0], kv_raw[1]
@@ -621,8 +656,6 @@
 
     finish(out_loads[0])
     y_copy(0).start()
-    finish(out_loads[1])
-    y_copy(1).start()
     finish(own_loads[1])
 
     @pl.when(is_mid)
@@ -634,12 +667,11 @@
         gain[:, i * 128 : (i + 1) * 128] = gain_raw[i : i + 1, :]
     tok_load.wait()
     norm_own()
-    for j in range(SUBS // 2):
+    for j in range(SUBS):
         tok_y(0, j).start()
-    finish(out_loads[2] + own_loads[2])
+    finish(out_loads[1] + out_loads[2] + own_loads[2])
+    y_copy(1).start()
     y_copy(2).start()
-    for j in range(SUBS // 2, SUBS):
-        tok_y(0, j).start()
 
     def relay(g, blk, onward):
         arrived(g, blk)
@@ -651,44 +683,49 @@
 
     def end_program():
         tok_z(0, 0).start()
+        make_bias()
         relay(0, theirs, to_pair)
         tok_z(0, 1).start()
         to_pair(1, mine).start()
-        relay(1, theirs, to_pair)
         tok_z(0, 2).start()
-        tok_z(0, 3).start()
-        to_pair(2, mine).start()
-        make_bias()
         take(0, 0)
         take(0, 1)
+        for blk in pt:
+            arrived(0, blk)
+        near(0, f)
         hand(0, 0)
-        relay(2, theirs, to_pair)
+        take(0, 2)
         hand(0, 1)
-        take(0, 2)
-        tok_z(1, 2).start()
+        take(0, 3)
         hand(0, 2)
-        take(0, 3)
-        tok_z(1, 3).start()
-        for blk in pt + ct + ft:
+        relay(1, theirs, to_pair)
+        tok_z(0, 3).start()
+        hand(0, 3)
+        for j in range(SUBS):
+            have(0, j)
+        near(0, other)
+        for blk in ct + ft:
             arrived(0, blk)
         project_qkv(f)
         kv_start(f, 0)
-        hand(0, 3)
-        for j in range(SUBS):
-            have(0, j)
         project_qkv(other)
         kv_start(other, 1)
+        to_pair(2, mine).start()
+        relay(2, theirs, to_pair)
+        tok_z(1, 2).start()
+        tok_z(1, 3).start()
         attend(f, 1, blocks - 2)
+        attend(other, 1, blocks - 2)
         kv_wait(f, 0)
         attend(f, 0, 2, blocks - 1)
         begin(attn_return(True))
-        attend(other, 1, blocks - 2)
         kv_wait(other, 1)
         attend(other, 0, 2, blocks - 1)
         begin(attn_return(False))
         for g in (1, 2):
-            for own_seq in (True, False):
-                conv_return(g, own_seq, False).wait_recv()
+            conv_return(g, True, False).wait_recv()
+            conv_return(g, False, False).wait_recv()
+            conv_return(g, False, False, 1).wait_recv()
         for g in range(GROUPS):
             to_pair(g, mine).wait_send()
             to_pair(g, theirs).wait_send()
@@ -702,102 +739,128 @@
         project_conv(g, seq, True)
         pr_start(g, seq, slot)
 
-    def conv_end(g, own_seq):
-        seq = f if own_seq else other
-        project_conv(g, seq, False)
-        mix(g, seq, False)
-        conv_return(g, own_seq, False).start()
-
     def conv_close(g, own_seq):
         seq, slot = (f, 0) if own_seq else (other, 1)
         pr_wait(g, seq, slot)
         mix(g, seq, True)
         conv_return(g, own_seq, True).start()
 
+    def conv_end(g):
+        project_conv(g, f, False)
+        mix(g, f, False)
+        conv_return(g, True, False).start()
+
+    def conv_end_head(g):
+        project_conv(g, other, False, 0, 1)
+        mix(g, other, False, 0, split)
+        conv_return(g, False, False).start()
+
+    def conv_end_tail(g):
+        project_conv(g, other, False, 1, 2)
+        mix(g, other, False, split, rows)
+        conv_return(g, False, False, 1).start()
+
     def mid_program():
+        half = (blocks - 2) // 2
         make_bias()
         relay(0, theirs, to_mid)
         to_pair(0, theirs).start()
-        relay(1, theirs, to_mid)
         relay(0, ct[0], to_pair)
         relay(0, pt[0], to_mid)
-        take(1, 0)
-        tok_y(1, 0).start()
         take(0, 0)
+        take(0, 1)
+        relay(0, ct[1], to_pair)
         relay(0, pt[1], to_mid)
         to_mid(2, mine).start()
-        relay(0, ct[1], to_pair)
-        hand(1, 0)
-        take(1, 1)
-        tok_y(1, 1).start()
-        take(0, 1)
+        near(0, f)
         hand(0, 0)
-        relay(2, theirs, to_mid)
-        relay(1, pt[0], to_mid)
-        hand(1, 1)
         relay(0, ft[0], to_pair)
-        take(2, 0)
+        take(0, 2)
         hand(0, 1)
-        relay(1, pt[1], to_mid)
+        take(0, 3)
+        take(1, 0)
         relay(0, ft[1], to_pair)
         project_qkv(f)
         kv_start(f, 0)
-        take(0, 2)
-        take(2, 1)
-        hand(2, 0)
-        attend(f, 1, (blocks - 2) // 2)
-        take(0, 3)
-        take(1, 2)
         hand(0, 2)
-        hand(2, 1)
-        attend(f, 1 + (blocks - 2) // 2, (blocks - 2) // 2)
-        take(1, 3)
+        take(1, 1)
+        relay(1, pt[0], to_mid)
+        attend(f, 1, half)
+        relay(1, theirs, to_mid)
         hand(0, 3)
-        hand(1, 2)
         for j in range(SUBS):
             have(0, j)
+        near(0, other)
         project_qkv(other)
         kv_start(other, 1)
-        relay(2, pt[0], to_mid)
-        hand(1, 3)
+        relay(2, theirs, to_mid)
+        take(1, 2)
+        attend(f, 1 + half, half)
+        hand(1, 0)
+        relay(1, pt[1], to_mid)
+        attend(other, 1, half)
+        near(1, f)
+        hand(1, 1)
+        near(1, other)
+        take(1, 3)
+        attend(other, 1 + half, half)
         kv_wait(f, 0)
         attend(f, 0, 2, blocks - 1)
         begin(attn_return(True))
-        relay(2, pt[1], to_mid)
-        attend(other, 1, blocks - 2)
+        hand(1, 2)
+        take(2, 0)
+        take(2, 1)
+        relay(2, pt[0], to_mid)
         kv_wait(other, 1)
         attend(other, 0, 2, blocks - 1)
         begin(attn_return(False))
         for blk in ct + ft:
             arrived(1, blk)
         conv_own(1, True)
+        hand(1, 3)
+        hand(2, 0)
         conv_own(1, False)
-        take(2, 2)
+        relay(2, pt[1], to_mid)
         for j in range(SUBS):
             have(1, j)
-        conv_end(1, True)
-        hand(2, 2)
-        take(2, 3)
+        near(1, 2 + f)
+        conv_end(1)
+        near(2, 2 + f)
+        hand(2, 1)
         conv_close(1, True)
-        hand(2, 3)
+        for j in range(SUBS // 2):
+            have(2, j)
+        near(1, 2 + other, 0, 1)
+        conv_end_head(1)
+        take(2, 2)
+        near(2, f)
+        near(2, other)
+        near(2, 2 + other, 0, 1)
         for blk in ct + ft:
             arrived(2, blk)
         conv_own(2, True)
+        take(2, 3)
         conv_own(2, False)
-        conv_end(2, True)
+        conv_end(2)
+        hand(2, 2)
+        conv_end_head(2)
         conv_close(2, True)
-        for j in range(SUBS):
+        hand(2, 3)
+        for j in range(SUBS // 2, SUBS):
             have(2, j)
-        conv_end(1, False)
-        conv_end(2, False)
+        near(1, 2 + other, 1, 2)
+        conv_end_tail(1)
+        near(2, 2 + other, 1, 2)
+        conv_end_tail(2)
         conv_close(1, False)
         conv_close(2, False)
         for g in (1, 2):
             conv_return(g, False, True).wait_recv()
             conv_return(g, True, True).wait()
             conv_return(g, False, True).wait_send()
-            for own_seq in (True, False):
-                conv_return(g, own_seq, False).wait_send()
+            conv_return(g, True, False).wait_send()
+            conv_return(g, False, False).wait_send()
+            conv_return(g, False, False, 1).wait_send()
         for blk in [mine, theirs] + ct + ft:
             to_pair(0, blk).wait_send()
         for g in range(GROUPS):
@@ -805,10 +868,12 @@
                 to_mid(g, blk).wait_send()
         for j in range(SUBS // 2):
             tok_y(1, j).wait_send()
+            tok_y(2, j).wait_send()
         for k in (1, 2):
             for j in range(SUBS):
                 for kind in range(3):
-                    tok_share(k, j, kind).wait_send()
+                    if k < 2 or j >= SUBS // 2 or kind != 1:
+                        tok_share(k, j, kind).wait_send()
 
     pl.when(is_end)(end_program)
     pl.when(is_mid)(mid_program)
@@ -869,6 +934,7 @@
             pltpu.VMEM((2, rows, qcols), bf),
             pltpu.VMEM((2, heads, rows), f32),
             pltpu.VMEM((2, 2, 2 * rows, chans), bf),
+            pltpu.VMEM((10, rows, group_cols), f32),
             pltpu.VMEM((2, depth, 2 * HEAD), bf),
             pltpu.VMEM((width // 128, 128), f32),
             pltpu.VMEM((1, width), f32),
@@ -883,7 +949,7 @@
             dma((GROUPS, 2 * SPAN)),
             dma((GROUPS, 2 * SPAN)),
             dma((GROUPS, 2 * SPAN)),
-            dma((2, SUBS)),
+            dma((3, SUBS)),
             dma((2, SUBS)),
             dma((3, SUBS, 3)),
             dma((3, SUBS, 4)),
@@ -893,8 +959,8 @@
             dma((2, 2)),
             dma((2,)),
             dma((2,)),
+            dma((2, 4)),
             dma((2, 3)),
-            dma((2, 2)),
         ],
         compiler_params=pltpu.CompilerParams(
             collective_id=0, has_side_effects=True, vmem_limit_bytes=67043328

time: 124 us -> 98.3 us (0.79)
  the two profiles are of different devices: /device:TPU:0 before, /device:TPU:17 now
where the time goes in v3:
time: 98.3 us; the launch traced here: 98.1 us
  Pallas kernels  92 us (94%)
  local copies, waits for them, and re-layouts  5.48 us (6%)
    pallas_call x1, Pallas kernels, fused_device(): pl.pallas_call(functools.partial(mega_kernel, tps), out_shape=(jax.ShapeD...  92 us
    unnamed x2, local copies, waits for them, and re-layouts  4.12 us

profile of v3, /device:TPU:17, one launch (start us, length us, event | category | flops | bytes accessed | tf_op | source)
XLA Modules:
  0.0 98.1 jit_solution(3852426984484872948)
XLA Ops:
  0.6 92.0 %shard_map.121 = (bf16[768,512]{1,0:T(8,128)(2,1)}, bf16[768,512]{1,0:T(8,128)(2,1)}, f32[2,4,768]{2,1,0:T(4,128)}) custom-call(bf16[768,2304]{1,0:T(8,128)(2,1)} %bitcast.4, f32[18,128]{1,0:T(8,128)} %bitcast.7, bf16[288,512]{1,0:T(8,128)(2,1)} %qw.1, bf16[288,128]{1,0:T(8,128)(2,1)} %kw.1, bf16[288,128]{1,0:T(8,128)(2,1)} %vw.1, bf16[288,512]{1,0:T(8,128)(2,1)} %ow.1, ...), custom_call_target="tpu_custom_call" | custom-call | tf_op jit(solution)/shard_map/pallas_call | solution.py:916
  92.6 1.4 %reshape.13 = f32[1,8,768]{2,1,0:T(8,128)} reshape(f32[2,4,768]{2,1,0:T(4,128)} %get-tuple-element.8) | data formatting | bytes 49152 | tf_op jit(solution)/shard_map/reshape | solution.py:980
  94.0 2.1 %copy.15 = bf16[1,768,512]{2,1,0:T(8,128)(2,1)} copy(bf16[1,768,512]{2,1,0:T(8,128)(2,1)} %bitcast.6) | data formatting | bytes 1572864
  96.0 2.1 %copy.16 = bf16[1,768,512]{2,1,0:T(8,128)(2,1)} copy(bf16[1,768,512]{2,1,0:T(8,128)(2,1)} %bitcast.5) | data formatting | bytes 1572864

commit v4 on v3

--- a/solution.py
+++ b/solution.py
@@ -339,7 +339,8 @@
         return (other, 2 + f, 2 + other)[k]
 
     def piece(slot, j, q):
-        return toks.at[slot, pl.ds(pl.multiple_of(j * sub + q * part, 16), part)]
+        place = jnp.where(low_half, SUBS - 1 - j, j)
+        return toks.at[slot, pl.ds(pl.multiple_of(place * sub + q * part, 16), part)]
 
     def tok_y(k, j):
         slot = f if k == 0 else 2 + f
@@ -420,8 +421,11 @@
     def sums(g, slot):
         return slot if g == 0 else slot + 4 * g - 2
 
-    def near(g, slot, lo=0, hi=2):
-        @pl.loop(lo, hi)
+    def halves_of(b):
+        return pl.loop(0, 2) if b is None else lambda body: body(b)
+
+    def near(g, slot, only=None):
+        @halves_of(only)
         def _(b):
             at = pl.multiple_of(b * mm_rows, WINDOW)
             acc[sums(g, slot), pl.ds(at, mm_rows), :] = partial(g, slot, at, near_k)
@@ -546,29 +550,34 @@
         return pl.ds(pl.multiple_of(f * (2 * chans) + (g - 1) * chans, 128), chans)
 
     split = mm_rows - pad
-
-    def conv_return(g, own_seq, own_rows, tail=0):
+    head_b = jnp.where(low_half, 1, 0)
+    spans = {
+        None: (0, rows),
+        "head": (jnp.where(low_half, rows - split, 0), split),
+        "tail": (jnp.where(low_half, 0, split), rows - split),
+    }
+
+    def conv_return(g, own_seq, own_rows, span=None):
         seq = f if own_seq else other
         off = own_off if own_rows else end_off
-        lo, count = 0, rows
-        if not own_seq and not own_rows:
-            lo, count = (split, rows - split) if tail else (0, split)
+        lo, count = spans[span]
         src = conv_st.at[g - 1, seq, pl.ds(pl.multiple_of(off + lo, pad), count)]
-        dst = conv_out.at[pl.ds(lo, count), conv_cols(g)]
+        dst = conv_out.at[pl.ds(pl.multiple_of(lo, pad), count), conv_cols(g)]
         if own_seq and own_rows:
             return pltpu.make_async_copy(src, dst, own_sem.at[g - 1])
         if own_seq:
             return remote(src, dst, conv_send.at[g - 1, 0], conv_recv.at[g - 1, 0], pair)
         if own_rows:
             return remote(src, dst, conv_send.at[g - 1, 1], conv_recv.at[g - 1, 1], across)
+        last = 1 if span == "tail" else 0
         return remote(
-            src, dst, conv_send.at[g - 1, 2 + tail], conv_recv.at[g - 1, 1 + tail], diag
-        )
-
-    def project_conv(g, seq, own_rows, lo=0, hi=2):
+            src, dst, conv_send.at[g - 1, 2 + last], conv_recv.at[g - 1, 1 + last], diag
+        )
+
+    def project_conv(g, seq, own_rows, only=None):
         slot, off = (seq, own_off) if own_rows else (2 + seq, end_off)
 
-        @pl.loop(lo, hi)
+        @halves_of(only)
         def _(b):
             at = pl.multiple_of(b * mm_rows, WINDOW)
             to = pl.multiple_of(off + b * mm_rows, WINDOW)
@@ -623,8 +632,8 @@
             fall.wait_send()
             climb.wait_recv()
 
-    def mix(g, seq, own_rows, lo=0, hi=None):
-        count = (rows if hi is None else hi) - lo
+    def mix(g, seq, own_rows, span=None):
+        lo, count = spans[span]
         off = pl.multiple_of((own_off if own_rows else end_off) + lo, pad)
         tap = taps[:, conv_cols(g)]
         size = count + 2 * pad
@@ -724,8 +733,8 @@
         begin(attn_return(False))
         for g in (1, 2):
             conv_return(g, True, False).wait_recv()
-            conv_return(g, False, False).wait_recv()
-            conv_return(g, False, False, 1).wait_recv()
+            conv_return(g, False, False, "head").wait_recv()
+            conv_return(g, False, False, "tail").wait_recv()
         for g in range(GROUPS):
             to_pair(g, mine).wait_send()
             to_pair(g, theirs).wait_send()
@@ -750,15 +759,10 @@
         mix(g, f, False)
         conv_return(g, True, False).start()
 
-    def conv_end_head(g):
-        project_conv(g, other, False, 0, 1)
-        mix(g, other, False, 0, split)
-        conv_return(g, False, False).start()
-
-    def conv_end_tail(g):
-        project_conv(g, other, False, 1, 2)
-        mix(g, other, False, split, rows)
-        conv_return(g, False, False, 1).start()
+    def conv_end_part(g, span):
+        project_conv(g, other, False, head_b if span == "head" else 1 - head_b)
+        mix(g, other, False, span)
+        conv_return(g, False, False, span).start()
 
     def mid_program():
         half = (blocks - 2) // 2
@@ -827,40 +831,40 @@
         conv_end(1)
         near(2, 2 + f)
         hand(2, 1)
+        take(2, 2)
         conv_close(1, True)
         for j in range(SUBS // 2):
             have(2, j)
-        near(1, 2 + other, 0, 1)
-        conv_end_head(1)
-        take(2, 2)
+        near(1, 2 + other, head_b)
+        conv_end_part(1, "head")
+        conv_close(1, False)
         near(2, f)
         near(2, other)
-        near(2, 2 + other, 0, 1)
+        take(2, 3)
+        near(2, 2 + other, head_b)
         for blk in ct + ft:
             arrived(2, blk)
         conv_own(2, True)
-        take(2, 3)
         conv_own(2, False)
+        hand(2, 2)
         conv_end(2)
-        hand(2, 2)
-        conv_end_head(2)
-        conv_close(2, True)
+        conv_end_part(2, "head")
+        conv_close(2, False)
         hand(2, 3)
         for j in range(SUBS // 2, SUBS):
             have(2, j)
-        near(1, 2 + other, 1, 2)
-        conv_end_tail(1)
-        near(2, 2 + other, 1, 2)
-        conv_end_tail(2)
-        conv_close(1, False)
-        conv_close(2, False)
+        near(1, 2 + other, 1 - head_b)
+        conv_end_part(1, "tail")
+        near(2, 2 + other, 1 - head_b)
+        conv_end_part(2, "tail")
+        conv_close(2, True)
         for g in (1, 2):
             conv_return(g, False, True).wait_recv()
             conv_return(g, True, True).wait()
             conv_return(g, False, True).wait_send()
             conv_return(g, True, False).wait_send()
-            conv_return(g, False, False).wait_send()
-            conv_return(g, False, False, 1).wait_send()
+            conv_return(g, False, False, "head").wait_send()
+            conv_return(g, False, False, "tail").wait_send()
         for blk in [mine, theirs] + ct + ft:
             to_pair(0, blk).wait_send()
         for g in range(GROUPS):
@@ -963,19 +967,24 @@
             dma((2, 3)),
         ],
         compiler_params=pltpu.CompilerParams(
-            collective_id=0, has_side_effects=True, vmem_limit_bytes=67043328
+            collective_id=0, has_side_effects=True, vmem_limit_bytes=48 << 20
         ),
     )(
-        tokens[0],
-        norm_gain.reshape(width // 128, 128),
-        query_weight,
-        key_weight,
-        value_weight,
-        outer_weight,
-        inner_weight,
-        signal_weight,
-        conv_taps,
-        sink_logit,
+        *(
+            pltpu.with_memory_space_constraint(x, pltpu.HBM)
+            for x in (
+                tokens[0],
+                norm_gain.reshape(width // 128, 128),
+                query_weight,
+                key_weight,
+                value_weight,
+                outer_weight,
+                inner_weight,
+                signal_weight,
+                conv_taps,
+                sink_logit,
+            )
+        )
     )
     return (attended[None], conv[None], logs.reshape(1, head_local, rows))
 

time: 98.3 us -> 90.5 us (0.921)
  the two profiles are of different devices: /device:TPU:17 before, /device:TPU:0 now
where the time goes in v4:
time: 90.5 us; the launch traced here: 90.4 us
  Pallas kernels  87.4 us (97%)
  local copies, waits for them, and re-layouts  2.38 us (3%)
    pallas_call x1, Pallas kernels, fused_device(): pl.pallas_call(functools.partial(mega_kernel, tps), out_shape=(jax.ShapeD...  87.4 us

profile of v4, /device:TPU:0, one launch (start us, length us, event | category | flops | bytes accessed | tf_op | source)
XLA Modules:
  0.0 90.4 jit_solution(14770763668252816926)
XLA Ops:
  0.6 87.4 %shard_map.121 = (bf16[768,512]{1,0:T(8,128)(2,1)S(1)}, bf16[768,512]{1,0:T(8,128)(2,1)S(1)}, f32[2,4,768]{2,1,0:T(4,128)S(1)}) custom-call(bf16[768,2304]{1,0:T(8,128)(2,1)} %bitcast.6, f32[18,128]{1,0:T(8,128)} %bitcast.7, bf16[288,512]{1,0:T(8,128)(2,1)} %qw.1, bf16[288,128]{1,0:T(8,128)(2,1)} %kw.1, bf16[288,128]{1,0:T(8,128)(2,1)} %vw.1, ...), custom_call_target="tpu_custom_call" | custom-call | tf_op jit(solution)/shard_map/pallas_call | solution.py:920
  88.0 0.6 reshape.13
  88.6 0.9 copy.15
  89.5 0.9 copy.16

commit v5 on v4

--- a/solution.py
+++ b/solution.py
@@ -166,6 +166,8 @@
 GROUPS = 3
 SPAN = 4
 SUBS = 4
+Y_PAIRS = 1
+Z_FIRST = 3
 FAR = -1e30
 
 
@@ -190,6 +192,7 @@
     qs,
     kvs,
     bias,
+    sink_row,
     prod,
     outer,
     attn_st,
@@ -214,6 +217,7 @@
     tok_z_send,
     tok_t_send,
     tok_recv,
+    tok_have,
     kv_send,
     kv_recv,
     pr_send,
@@ -273,13 +277,16 @@
                 (ref.at[:, c], dest.at[:, pl.ds(i * chans, chans)])
                 for i, ref in enumerate((iw, sw, ow))
             ]
-        return [
-            pltpu.make_async_copy(a, b, sems.at[g, i]) for i, (a, b) in enumerate(pairs)
-        ]
+        return [pltpu.make_async_copy(a, b, sems.at[g]) for a, b in pairs]
+
+    def loaded(g, dest, sems):
+        whole = dest.at[:, pl.ds(0, qcols)] if g == 0 else dest
+        pltpu.make_async_copy(whole, whole, sems.at[g]).wait()
 
     mine = s * 2 + f
     theirs = s * 2 + other
-    own_loads = [loads(g, f, wts.at[g, block_rows(mine)], load_sem) for g in range(GROUPS)]
+    own_dest = [wts.at[g, block_rows(mine)] for g in range(GROUPS)]
+    own_loads = [loads(g, f, own_dest[g], load_sem) for g in range(GROUPS)]
     out_loads = [loads(g, other, stage_w.at[g], stage_sem) for g in range(GROUPS)]
     small = [
         pltpu.make_async_copy(a, b, small_sem.at[i])
@@ -322,15 +329,19 @@
             stage_w.at[g], wts.at[g, block_rows(mine)], y_send.at[g], w_recv.at[g, mine], across
         )
 
-    def block_copy(g, blk, sends, peer):
+    def block_copy(g, blk, send, peer):
         at = wts.at[g, block_rows(blk)]
-        return remote(at, at, sends.at[g, blk], w_recv.at[g, blk], peer)
+        return remote(at, at, send, w_recv.at[g, blk], peer)
 
     def to_pair(g, blk):
-        return block_copy(g, blk, pair_send, pair)
+        return block_copy(g, blk, pair_send.at[0], pair)
 
     def to_mid(g, blk):
-        return block_copy(g, blk, mid_send, mid)
+        return block_copy(g, blk, mid_send.at[g], mid)
+
+    def blocks_sent(send, count):
+        at = wts.at[0, pl.ds(0, count * depth)]
+        remote(at, at, send, w_recv.at[0, 0], across).wait_send()
 
     def arrived(g, blk):
         to_pair(g, blk).wait_recv()
@@ -345,48 +356,50 @@
     def tok_y(k, j):
         slot = f if k == 0 else 2 + f
         at = piece(slot, j, beyond_t if k == 2 else t)
-        kind = 2 if k == 2 else 0
-        return remote(at, at, tok_y_send.at[k, j], tok_recv.at[2 if k else 0, j, kind], across)
+        return remote(
+            at, at, tok_y_send.at[1 if k else 0], tok_recv.at[2 if k else 0, j, k // 2], across
+        )
 
     def tok_z(k, j):
         seq = f if k == 0 else other
         return remote(
-            piece(seq, j, t),
-            piece(2 + seq, j, t),
-            tok_z_send.at[k, j],
-            tok_recv.at[1 + k, j, 0],
-            pair,
-        )
+            piece(seq, j, t), piece(2 + seq, j, t), tok_z_send.at[0], tok_recv.at[1 + k, j, 0], pair
+        )
+
+    def have_slot(k, j):
+        if k == 0:
+            return j // (SUBS // 2)
+        return 2 if k == 1 else 3 + max(0, j - 1)
 
     def tok_share(k, j, kind):
-        q = beyond_t if kind == 2 else t
-        at = piece(slot_of(k), j, q)
-        return remote(
-            at, at, tok_t_send.at[k, j, kind], tok_recv.at[k, j, kind + 1],
-            beyond if kind == 1 else mate,
-        )
+        at = piece(slot_of(k), j, beyond_t if kind == 2 else t)
+        if kind == 1:
+            return remote(at, at, tok_t_send.at[k], tok_recv.at[k, j, 1], beyond)
+        return remote(at, at, tok_t_send.at[k], tok_have.at[have_slot(k, j)], mate)
 
     def tok_wait(k, j, kind):
         at = piece(slot_of(k), j, t)
-        remote(at, at, tok_t_send.at[k, j, 0], tok_recv.at[k, j, kind], mate).wait_recv()
+        remote(at, at, tok_t_send.at[k], tok_recv.at[k, j, kind], mate).wait_recv()
 
     def take(k, j):
         tok_wait(k, j, 0)
-        if k < 2 or j >= SUBS // 2:
+        if k < 2 or j >= Y_PAIRS:
             tok_share(k, j, 1).start()
         tok_share(k, j, 0).start()
-        if k == 1 and j < SUBS // 2:
+        if k == 1 and j < Z_FIRST:
             tok_y(1, j).start()
 
     def hand(k, j):
-        tok_wait(k, j, 2)
+        tok_wait(k, j, 1)
         tok_share(k, j, 2).start()
-        if k == 1 and j < SUBS // 2:
-            tok_y(2, j).start()
-
-    def have(k, j):
-        tok_wait(k, j, 1)
-        tok_wait(k, j, 3)
+
+    def have(index, pieces):
+        at = toks.at[0, pl.ds(0, pieces * part)]
+        remote(at, at, tok_t_send.at[0], tok_have.at[index], mate).wait_recv()
+
+    def pieces_sent(send, pieces):
+        at = toks.at[0, pl.ds(0, pieces * part)]
+        remote(at, at, send, tok_have.at[0], mate).wait_send()
 
     def norm_own():
         @pl.loop(0, blocks)
@@ -405,8 +418,11 @@
         for h in range(heads):
             index = (t * (2 * heads) + f * heads + h + 1).astype(jnp.float32)
             slope = jnp.exp2(jnp.full((1, WINDOW), -8.0 / (2 * heads * tps), jnp.float32) * index)
-            bias[h] = jnp.where(away <= WINDOW, -slope * away.astype(jnp.float32), FAR)
-
+            cols = pl.ds(h * WINDOW, WINDOW)
+            bias[:, cols] = jnp.where(away <= WINDOW, -slope * away.astype(jnp.float32), FAR)
+            sink_row[:, cols] = jnp.full((1, WINDOW), sinks[f * heads + h], jnp.float32)
+
+    scale = 1.0 / math.sqrt(HEAD)
     half_k = depth * SPAN
     near_k = pl.multiple_of(jnp.where(low_half, 0, half_k), 128)
     far_k = pl.multiple_of(half_k - near_k, 128)
@@ -438,7 +454,7 @@
         def _(b):
             at = pl.multiple_of(b * mm_rows, WINDOW)
             out = total(0, seq, at)
-            qs[seq, pl.ds(at, mm_rows), :] = out[:, :qcols].astype(jnp.bfloat16)
+            qs[seq, pl.ds(at, mm_rows), :] = (out[:, :qcols] * scale).astype(jnp.bfloat16)
             kvs[seq, pl.ds(at + WINDOW, mm_rows), :] = out[:, qcols:].astype(jnp.bfloat16)
 
     kv_len = kvs.shape[1]
@@ -494,7 +510,7 @@
             fall.wait_send()
             climb.wait_recv()
 
-    def attend(seq, first, count, step=1):
+    def attend(seq, first, count, step=1, closed=False):
         @pl.loop(0, count)
         def _(i):
             b = first + i * step
@@ -503,15 +519,16 @@
             keys = kv[:, :HEAD]
             values_t = kv.astype(jnp.float32).T[HEAD:, :].astype(jnp.bfloat16)
             queries = qs[seq, pl.ds(at, WINDOW), :]
-            low = jnp.where((b == 0) & (s == 0), FAR, 0.0)
-            high = jnp.where((b == blocks - 1) & (s == SPAN - 1), FAR, 0.0)
-            outs = []
-            for h in range(heads):
-                query = queries[:, h * HEAD : (h + 1) * HEAD]
-                scores = lax.dot_general(
-                    keys, query, (((1,), (1,)), ((), ())), preferred_element_type=jnp.float32
-                )
-                scores = scores * (1.0 / math.sqrt(HEAD)) + bias[h]
+            stacked = jnp.concatenate(
+                [queries[:, h * HEAD : (h + 1) * HEAD] for h in range(heads)], axis=0
+            )
+            scores = lax.dot_general(
+                keys, stacked, (((1,), (1,)), ((), ())), preferred_element_type=jnp.float32
+            )
+            scores = scores + bias[...]
+            if closed:
+                low = jnp.where((b == 0) & (s == 0), FAR, 0.0)
+                high = jnp.where((b == blocks - 1) & (s == SPAN - 1), FAR, 0.0)
                 scores = jnp.concatenate(
                     [
                         scores[:WINDOW] + low,
@@ -520,17 +537,23 @@
                     ],
                     axis=0,
                 )
-                sink = sinks[f * heads + h]
-                peak = jnp.maximum(jnp.max(scores, axis=0, keepdims=True), sink)
-                weights = jnp.exp(scores - peak)
-                total = jnp.sum(weights, axis=0, keepdims=True) + jnp.exp(sink - peak)
-                mixed = jnp.dot(
-                    values_t, weights.astype(jnp.bfloat16), preferred_element_type=jnp.float32
-                )
-                outs.append(mixed / total)
-                log_st[seq, pl.ds(h, 1), pl.ds(at, WINDOW)] = peak + jnp.log(total)
-            stacked = jnp.concatenate(outs, axis=0)
-            attn_st[seq, pl.ds(at, WINDOW), :] = stacked.T.astype(jnp.bfloat16)
+            sink = sink_row[...]
+            peak = jnp.maximum(jnp.max(scores, axis=0, keepdims=True), sink)
+            weights = jnp.exp(scores - peak)
+            total = jnp.sum(weights, axis=0, keepdims=True) + jnp.exp(sink - peak)
+            mixed = jnp.dot(
+                values_t, weights.astype(jnp.bfloat16), preferred_element_type=jnp.float32
+            )
+            mixed = mixed / total
+            logs = peak + jnp.log(total)
+            outs = []
+            for h in range(heads):
+                cols = slice(h * WINDOW, (h + 1) * WINDOW)
+                outs.append(mixed[:, cols])
+                log_st[seq, pl.ds(h, 1), pl.ds(at, WINDOW)] = logs[:, cols]
+            attn_st[seq, pl.ds(at, WINDOW), :] = (
+                jnp.concatenate(outs, axis=0).T.astype(jnp.bfloat16)
+            )
 
     half_cols = pl.ds(pl.multiple_of(f * qcols, 128), qcols)
 
@@ -587,6 +610,17 @@
             prod[g - 1, seq, pl.ds(to + pad, mm_rows), :] = (inner * signal).astype(jnp.bfloat16)
             outer[g - 1, seq, pl.ds(to, mm_rows), :] = out[:, 2 * chans :].astype(jnp.bfloat16)
 
+    def project_tail(g, j):
+        at = pl.multiple_of(jnp.where(low_half, SUBS - 1 - j, j) * sub, 16)
+        out = jnp.dot(
+            toks[2 + other, pl.ds(at, sub), :], wts[g], preferred_element_type=jnp.float32
+        )
+        inner = out[:, :chans].astype(jnp.bfloat16).astype(jnp.float32)
+        signal = out[:, chans : 2 * chans].astype(jnp.bfloat16).astype(jnp.float32)
+        to = pl.multiple_of(end_off + at, 16)
+        prod[g - 1, other, pl.ds(to + pad, sub), :] = (inner * signal).astype(jnp.bfloat16)
+        outer[g - 1, other, pl.ds(to, sub), :] = out[:, 2 * chans :].astype(jnp.bfloat16)
+
     def pr_copies(g, seq, slot):
         ref = prod.at[g - 1, seq]
         climb = remote(
@@ -656,16 +690,22 @@
 
     pl.semaphore_wait(barrier, jnp.where(is_mid, 6, 5))
 
-    finish(own_loads[0])
+    loaded(0, own_dest[0], load_sem)
     to_pair(0, mine).start()
 
     @pl.when(is_mid)
     def _():
         to_mid(0, mine).start()
 
-    finish(out_loads[0])
-    y_copy(0).start()
-    finish(own_loads[1])
+    loaded(0, stage_w.at[0], stage_sem)
+    loaded(1, stage_w.at[1], stage_sem)
+
+    @pl.when(is_end)
+    def _():
+        y_copy(0).start()
+        y_copy(1).start()
+
+    loaded(1, own_dest[1], load_sem)
 
     @pl.when(is_mid)
     def _():
@@ -676,11 +716,22 @@
         gain[:, i * 128 : (i + 1) * 128] = gain_raw[i : i + 1, :]
     tok_load.wait()
     norm_own()
-    for j in range(SUBS):
+    tok_y(0, 0).start()
+
+    @pl.when(is_mid)
+    def _():
+        y_copy(0).start()
+
+    for j in range(1, SUBS):
         tok_y(0, j).start()
-    finish(out_loads[1] + out_loads[2] + own_loads[2])
-    y_copy(1).start()
+
+    @pl.when(is_mid)
+    def _():
+        y_copy(1).start()
+
+    loaded(2, stage_w.at[2], stage_sem)
     y_copy(2).start()
+    loaded(2, own_dest[2], load_sem)
 
     def relay(g, blk, onward):
         arrived(g, blk)
@@ -696,52 +747,48 @@
         relay(0, theirs, to_pair)
         tok_z(0, 1).start()
         to_pair(1, mine).start()
+        relay(1, theirs, to_pair)
         tok_z(0, 2).start()
+        tok_z(0, 3).start()
         take(0, 0)
-        take(0, 1)
         for blk in pt:
             arrived(0, blk)
         near(0, f)
+        take(0, 1)
         hand(0, 0)
         take(0, 2)
         hand(0, 1)
         take(0, 3)
         hand(0, 2)
-        relay(1, theirs, to_pair)
-        tok_z(0, 3).start()
-        hand(0, 3)
-        for j in range(SUBS):
-            have(0, j)
-        near(0, other)
+        have(0, 2 * (SUBS // 2))
+        near(0, other, head_b)
         for blk in ct + ft:
             arrived(0, blk)
         project_qkv(f)
         kv_start(f, 0)
+        to_pair(2, mine).start()
+        hand(0, 3)
+        have(1, 2 * (SUBS // 2))
+        near(0, other, 1 - head_b)
         project_qkv(other)
         kv_start(other, 1)
-        to_pair(2, mine).start()
         relay(2, theirs, to_pair)
-        tok_z(1, 2).start()
-        tok_z(1, 3).start()
+        for j in range(Z_FIRST, SUBS):
+            tok_z(1, j).start()
         attend(f, 1, blocks - 2)
         attend(other, 1, blocks - 2)
         kv_wait(f, 0)
-        attend(f, 0, 2, blocks - 1)
+        attend(f, 0, 2, blocks - 1, True)
         begin(attn_return(True))
         kv_wait(other, 1)
-        attend(other, 0, 2, blocks - 1)
+        attend(other, 0, 2, blocks - 1, True)
         begin(attn_return(False))
         for g in (1, 2):
             conv_return(g, True, False).wait_recv()
             conv_return(g, False, False, "head").wait_recv()
             conv_return(g, False, False, "tail").wait_recv()
-        for g in range(GROUPS):
-            to_pair(g, mine).wait_send()
-            to_pair(g, theirs).wait_send()
-        for j in range(SUBS):
-            tok_z(0, j).wait_send()
-        for j in range(SUBS // 2, SUBS):
-            tok_z(1, j).wait_send()
+        blocks_sent(pair_send.at[0], 2 * GROUPS)
+        pieces_sent(tok_z_send.at[0], 2 * SUBS - Z_FIRST)
 
     def conv_own(g, own_seq):
         seq, slot = (f, 0) if own_seq else (other, 1)
@@ -759,104 +806,107 @@
         mix(g, f, False)
         conv_return(g, True, False).start()
 
-    def conv_end_part(g, span):
-        project_conv(g, other, False, head_b if span == "head" else 1 - head_b)
+    def conv_end_close(g, span):
         mix(g, other, False, span)
         conv_return(g, False, False, span).start()
 
     def mid_program():
         half = (blocks - 2) // 2
         make_bias()
-        relay(0, theirs, to_mid)
-        to_pair(0, theirs).start()
         relay(0, ct[0], to_pair)
         relay(0, pt[0], to_mid)
         take(0, 0)
-        take(0, 1)
-        relay(0, ct[1], to_pair)
+        take(1, 0)
+        relay(0, theirs, to_mid)
+        to_pair(0, theirs).start()
+        hand(0, 0)
         relay(0, pt[1], to_mid)
         to_mid(2, mine).start()
         near(0, f)
-        hand(0, 0)
+        take(0, 1)
+        relay(0, ct[1], to_pair)
+        hand(1, 0)
+        take(0, 2)
         relay(0, ft[0], to_pair)
-        take(0, 2)
+        take(1, 1)
         hand(0, 1)
+        have(0, 2 * (SUBS // 2))
+        near(0, other, head_b)
+        relay(0, ft[1], to_pair)
         take(0, 3)
-        take(1, 0)
-        relay(0, ft[1], to_pair)
+        relay(1, pt[0], to_mid)
         project_qkv(f)
         kv_start(f, 0)
         hand(0, 2)
-        take(1, 1)
-        relay(1, pt[0], to_mid)
         attend(f, 1, half)
         relay(1, theirs, to_mid)
+        attend(f, 1 + half, half)
+        relay(1, pt[1], to_mid)
+        near(1, f)
         hand(0, 3)
-        for j in range(SUBS):
-            have(0, j)
-        near(0, other)
+        have(1, 2 * (SUBS // 2))
+        near(0, other, 1 - head_b)
         project_qkv(other)
         kv_start(other, 1)
         relay(2, theirs, to_mid)
         take(1, 2)
-        attend(f, 1 + half, half)
-        hand(1, 0)
-        relay(1, pt[1], to_mid)
+        tok_y(2, 0).start()
         attend(other, 1, half)
-        near(1, f)
         hand(1, 1)
+        attend(other, 1 + half, half)
         near(1, other)
         take(1, 3)
-        attend(other, 1 + half, half)
         kv_wait(f, 0)
         attend(f, 0, 2, blocks - 1)
         begin(attn_return(True))
         hand(1, 2)
         take(2, 0)
+        relay(2, pt[0], to_mid)
+        for blk in ct + ft:
+            arrived(1, blk)
+        conv_own(1, True)
         take(2, 1)
-        relay(2, pt[0], to_mid)
+        conv_own(1, False)
         kv_wait(other, 1)
         attend(other, 0, 2, blocks - 1)
         begin(attn_return(False))
-        for blk in ct + ft:
-            arrived(1, blk)
-        conv_own(1, True)
         hand(1, 3)
-        hand(2, 0)
-        conv_own(1, False)
         relay(2, pt[1], to_mid)
-        for j in range(SUBS):
-            have(1, j)
+        have(2, 2 * SUBS)
         near(1, 2 + f)
+        take(2, 2)
         conv_end(1)
         near(2, 2 + f)
+        conv_close(1, True)
         hand(2, 1)
-        take(2, 2)
-        conv_close(1, True)
-        for j in range(SUBS // 2):
-            have(2, j)
+        near(2, f)
+        hand(2, 0)
+        take(2, 3)
+        have(3, 4)
         near(1, 2 + other, head_b)
-        conv_end_part(1, "head")
+        project_conv(1, other, False, head_b)
+        conv_end_close(1, "head")
         conv_close(1, False)
-        near(2, f)
         near(2, other)
-        take(2, 3)
+        hand(2, 2)
         near(2, 2 + other, head_b)
         for blk in ct + ft:
             arrived(2, blk)
         conv_own(2, True)
+        conv_end(2)
+        have(4, 2)
+        project_tail(1, 2)
+        hand(2, 3)
         conv_own(2, False)
-        hand(2, 2)
-        conv_end(2)
-        conv_end_part(2, "head")
+        project_conv(2, other, False, head_b)
+        conv_end_close(2, "head")
         conv_close(2, False)
-        hand(2, 3)
-        for j in range(SUBS // 2, SUBS):
-            have(2, j)
-        near(1, 2 + other, 1 - head_b)
-        conv_end_part(1, "tail")
-        near(2, 2 + other, 1 - head_b)
-        conv_end_part(2, "tail")
+        have(5, 2)
+        project_tail(1, 3)
+        conv_end_close(1, "tail")
+        project_tail(2, 2)
+        project_tail(2, 3)
+        conv_end_close(2, "tail")
         conv_close(2, True)
         for g in (1, 2):
             conv_return(g, False, True).wait_recv()
@@ -865,29 +915,19 @@
             conv_return(g, True, False).wait_send()
             conv_return(g, False, False, "head").wait_send()
             conv_return(g, False, False, "tail").wait_send()
-        for blk in [mine, theirs] + ct + ft:
-            to_pair(0, blk).wait_send()
+            pieces_sent(tok_t_send.at[g], 3 * SUBS if g == 1 else 3 * SUBS - Y_PAIRS)
+        blocks_sent(pair_send.at[0], 6)
         for g in range(GROUPS):
-            for blk in [mine, theirs] + pt:
-                to_mid(g, blk).wait_send()
-        for j in range(SUBS // 2):
-            tok_y(1, j).wait_send()
-            tok_y(2, j).wait_send()
-        for k in (1, 2):
-            for j in range(SUBS):
-                for kind in range(3):
-                    if k < 2 or j >= SUBS // 2 or kind != 1:
-                        tok_share(k, j, kind).wait_send()
+            blocks_sent(mid_send.at[g], 4)
+        pieces_sent(tok_y_send.at[1], Z_FIRST + Y_PAIRS)
 
     pl.when(is_end)(end_program)
     pl.when(is_mid)(mid_program)
 
     for g in range(GROUPS):
         y_copy(g).wait_send()
-    for j in range(SUBS):
-        tok_y(0, j).wait_send()
-        for kind in range(3):
-            tok_share(0, j, kind).wait_send()
+    pieces_sent(tok_y_send.at[0], SUBS)
+    pieces_sent(tok_t_send.at[0], 3 * SUBS)
     for own in (True, False):
         finish(attn_return(own))
 
@@ -932,7 +972,8 @@
             pltpu.VMEM((GROUPS, depth, group_cols), bf),
             pltpu.VMEM((2, rows, qcols), bf),
             pltpu.VMEM((2, rows + 2 * WINDOW, 2 * HEAD), bf),
-            pltpu.VMEM((heads, 3 * WINDOW, WINDOW), f32),
+            pltpu.VMEM((3 * WINDOW, heads * WINDOW), f32),
+            pltpu.VMEM((1, heads * WINDOW), f32),
             pltpu.VMEM((2, 2, 2 * rows + 2 * pad, chans), bf),
             pltpu.VMEM((2, 2, 2 * rows, chans), bf),
             pltpu.VMEM((2, rows, qcols), bf),
@@ -945,18 +986,19 @@
             pltpu.VMEM((3, 4 * chans), f32),
             pltpu.SMEM((head_local,), f32),
             dma((5,)),
-            dma((GROUPS, 3)),
-            dma((GROUPS, 3)),
+            dma((GROUPS,)),
+            dma((GROUPS,)),
             dma((3,)),
             dma((2,)),
             dma((GROUPS,)),
             dma((GROUPS, 2 * SPAN)),
-            dma((GROUPS, 2 * SPAN)),
-            dma((GROUPS, 2 * SPAN)),
-            dma((3, SUBS)),
-            dma((2, SUBS)),
-            dma((3, SUBS, 3)),
-            dma((3, SUBS, 4)),
+            dma((1,)),
+            dma((GROUPS,)),
+            dma((2,)),
+            dma((1,)),
+            dma((3,)),
+            dma((3, SUBS, 2)),
+            dma((6,)),
             dma((2, 2)),
             dma((2, 2)),
             dma((2, 2)),

time: 90.5 us -> 87.4 us (0.966)
  Pallas kernels: 87.4 us -> 84.2 us
    pallas_call x1, Pallas kernels: 87.4 us -> 84.2 us  [fused_device(): pl.pallas_call(functools.partial(mega_kernel, tps), out_shape=(jax.ShapeD...]
where the time goes in v5:
time: 87.4 us; the launch traced here: 87.2 us
  Pallas kernels  84.2 us (96%)
  local copies, waits for them, and re-layouts  2.38 us (3%)
    pallas_call x1, Pallas kernels, fused_device(): pl.pallas_call(functools.partial(mega_kernel, tps), out_shape=(jax.ShapeD...  84.2 us
    unnamed x2, local copies, waits for them, and re-layouts  1.76 us

profile of v5, /device:TPU:0, one launch (start us, length us, event | category | flops | bytes accessed | tf_op | source)
XLA Modules:
  0.0 87.2 jit_solution(13240795755383603644)
XLA Ops:
  0.6 84.2 %shard_map.121 = (bf16[768,512]{1,0:T(8,128)(2,1)S(1)}, bf16[768,512]{1,0:T(8,128)(2,1)S(1)}, f32[2,4,768]{2,1,0:T(4,128)S(1)}) custom-call(bf16[768,2304]{1,0:T(8,128)(2,1)} %bitcast.6, f32[18,128]{1,0:T(8,128)} %bitcast.7, bf16[288,512]{1,0:T(8,128)(2,1)} %qw.1, bf16[288,128]{1,0:T(8,128)(2,1)} %kw.1, bf16[288,128]{1,0:T(8,128)(2,1)} %vw.1, ...), custom_call_target="tpu_custom_call" | custom-call | tf_op jit(solution)/shard_map/pallas_call | solution.py:960
  84.8 0.6 reshape.13
  85.5 0.9 %copy.15 = bf16[1,768,512]{2,1,0:T(8,128)(2,1)} copy(bf16[1,768,512]{2,1,0:T(8,128)(2,1)S(1)} %bitcast.5) | data formatting | bytes 1572864
  86.3 0.9 %copy.16 = bf16[1,768,512]{2,1,0:T(8,128)(2,1)} copy(bf16[1,768,512]{2,1,0:T(8,128)(2,1)S(1)} %bitcast.4) | data formatting | bytes 1572864

commit v6 on v5

--- a/solution.py
+++ b/solution.py
@@ -367,9 +367,9 @@
         )
 
     def have_slot(k, j):
-        if k == 0:
-            return j // (SUBS // 2)
-        return 2 if k == 1 else 3 + max(0, j - 1)
+        if k < 2:
+            return 2 * k + j // (SUBS // 2)
+        return 4 + max(0, j - 1)
 
     def tok_share(k, j, kind):
         at = piece(slot_of(k), j, beyond_t if kind == 2 else t)
@@ -438,7 +438,9 @@
         return slot if g == 0 else slot + 4 * g - 2
 
     def halves_of(b):
-        return pl.loop(0, 2) if b is None else lambda body: body(b)
+        if b is None:
+            return lambda body: [body(i) for i in range(2)]
+        return lambda body: body(b)
 
     def near(g, slot, only=None):
         @halves_of(only)
@@ -511,8 +513,7 @@
             climb.wait_recv()
 
     def attend(seq, first, count, step=1, closed=False):
-        @pl.loop(0, count)
-        def _(i):
+        def block(i):
             b = first + i * step
             at = pl.multiple_of(b * WINDOW, WINDOW)
             kv = kvs[seq, pl.ds(at, 3 * WINDOW), :]
@@ -555,6 +556,11 @@
                 jnp.concatenate(outs, axis=0).T.astype(jnp.bfloat16)
             )
 
+        @pl.loop(0, count // 2)
+        def _(i):
+            block(2 * i)
+            block(2 * i + 1)
+
     half_cols = pl.ds(pl.multiple_of(f * qcols, 128), qcols)
 
     def attn_return(own):
@@ -589,12 +595,13 @@
         if own_seq and own_rows:
             return pltpu.make_async_copy(src, dst, own_sem.at[g - 1])
         if own_seq:
-            return remote(src, dst, conv_send.at[g - 1, 0], conv_recv.at[g - 1, 0], pair)
+            last = 3 if span == "tail" else 0
+            return remote(src, dst, conv_send.at[g - 1, last], conv_recv.at[g - 1, last], pair)
         if own_rows:
             return remote(src, dst, conv_send.at[g - 1, 1], conv_recv.at[g - 1, 1], across)
         last = 1 if span == "tail" else 0
         return remote(
-            src, dst, conv_send.at[g - 1, 2 + last], conv_recv.at[g - 1, 1 + last], diag
+            src, dst, conv_send.at[g - 1, 2 + 2 * last], conv_recv.at[g - 1, 1 + last], diag
         )
 
     def project_conv(g, seq, own_rows, only=None):
@@ -639,19 +646,23 @@
         )
         return climb, fall
 
+    def pr_blank():
+        place = pl.multiple_of(jnp.where(low_half, 0, both_rows + pad), pad)
+        blank = jnp.zeros((pad, chans), jnp.bfloat16)
+        for g in range(2):
+            for seq in range(2):
+                prod[g, seq, pl.ds(place, pad), :] = blank
+
     def pr_start(g, seq, slot):
         climb, fall = pr_copies(g, seq, slot)
-        blank = jnp.zeros((pad, chans), jnp.bfloat16)
 
         @pl.when(low_half)
         def _():
             climb.start()
-            prod[g - 1, seq, pl.ds(0, pad), :] = blank
 
         @pl.when(jnp.logical_not(low_half))
         def _():
             fall.start()
-            prod[g - 1, seq, pl.ds(both_rows + pad, pad), :] = blank
 
     def pr_wait(g, seq, slot):
         climb, fall = pr_copies(g, seq, slot)
@@ -745,11 +756,10 @@
         tok_z(0, 0).start()
         make_bias()
         relay(0, theirs, to_pair)
-        tok_z(0, 1).start()
         to_pair(1, mine).start()
         relay(1, theirs, to_pair)
-        tok_z(0, 2).start()
-        tok_z(0, 3).start()
+        for j in range(1, SUBS):
+            tok_z(0, j).start()
         take(0, 0)
         for blk in pt:
             arrived(0, blk)
@@ -784,7 +794,8 @@
         attend(other, 0, 2, blocks - 1, True)
         begin(attn_return(False))
         for g in (1, 2):
-            conv_return(g, True, False).wait_recv()
+            for span in (None,) if g == 1 else ("head", "tail"):
+                conv_return(g, True, False, span).wait_recv()
             conv_return(g, False, False, "head").wait_recv()
             conv_return(g, False, False, "tail").wait_recv()
         blocks_sent(pair_send.at[0], 2 * GROUPS)
@@ -801,8 +812,7 @@
         mix(g, seq, True)
         conv_return(g, own_seq, True).start()
 
-    def conv_end(g):
-        project_conv(g, f, False)
+    def conv_close_end(g):
         mix(g, f, False)
         conv_return(g, True, False).start()
 
@@ -813,106 +823,119 @@
     def mid_program():
         half = (blocks - 2) // 2
         make_bias()
+        pr_blank()
         relay(0, ct[0], to_pair)
         relay(0, pt[0], to_mid)
         take(0, 0)
         take(1, 0)
         relay(0, theirs, to_mid)
         to_pair(0, theirs).start()
-        hand(0, 0)
         relay(0, pt[1], to_mid)
-        to_mid(2, mine).start()
         near(0, f)
         take(0, 1)
+        hand(0, 0)
         relay(0, ct[1], to_pair)
-        hand(1, 0)
+        relay(1, pt[0], to_mid)
         take(0, 2)
         relay(0, ft[0], to_pair)
-        take(1, 1)
         hand(0, 1)
         have(0, 2 * (SUBS // 2))
         near(0, other, head_b)
+        hand(1, 0)
         relay(0, ft[1], to_pair)
         take(0, 3)
-        relay(1, pt[0], to_mid)
+        relay(1, pt[1], to_mid)
         project_qkv(f)
         kv_start(f, 0)
+        attend(f, 1, half)
+        attend(f, 1 + half, half)
+        take(1, 1)
         hand(0, 2)
-        attend(f, 1, half)
         relay(1, theirs, to_mid)
-        attend(f, 1 + half, half)
-        relay(1, pt[1], to_mid)
+        to_mid(2, mine).start()
         near(1, f)
         hand(0, 3)
         have(1, 2 * (SUBS // 2))
         near(0, other, 1 - head_b)
         project_qkv(other)
         kv_start(other, 1)
-        relay(2, theirs, to_mid)
         take(1, 2)
         tok_y(2, 0).start()
         attend(other, 1, half)
-        hand(1, 1)
         attend(other, 1 + half, half)
         near(1, other)
+        relay(2, theirs, to_mid)
         take(1, 3)
+        for blk in ct + ft:
+            arrived(1, blk)
+        conv_own(1, True)
+        conv_own(1, False)
         kv_wait(f, 0)
         attend(f, 0, 2, blocks - 1)
         begin(attn_return(True))
-        hand(1, 2)
+        hand(1, 1)
+        have(2, 2 * (SUBS // 2))
+        near(1, 2 + f, head_b)
+        relay(2, pt[0], to_mid)
         take(2, 0)
-        relay(2, pt[0], to_mid)
-        for blk in ct + ft:
-            arrived(1, blk)
-        conv_own(1, True)
         take(2, 1)
-        conv_own(1, False)
+        project_conv(1, f, False, head_b)
         kv_wait(other, 1)
         attend(other, 0, 2, blocks - 1)
         begin(attn_return(False))
+        hand(1, 2)
         hand(1, 3)
+        have(3, 2 * (SUBS // 2))
+        near(1, 2 + f, 1 - head_b)
         relay(2, pt[1], to_mid)
-        have(2, 2 * SUBS)
-        near(1, 2 + f)
         take(2, 2)
-        conv_end(1)
+        project_conv(1, f, False, 1 - head_b)
+        conv_close_end(1)
+        near(2, f)
+        near(2, other)
         near(2, 2 + f)
         conv_close(1, True)
+        hand(2, 0)
         hand(2, 1)
-        near(2, f)
-        hand(2, 0)
         take(2, 3)
-        have(3, 4)
+        have(4, 4)
         near(1, 2 + other, head_b)
         project_conv(1, other, False, head_b)
         conv_end_close(1, "head")
         conv_close(1, False)
-        near(2, other)
-        hand(2, 2)
         near(2, 2 + other, head_b)
         for blk in ct + ft:
             arrived(2, blk)
-        conv_own(2, True)
-        conv_end(2)
-        have(4, 2)
-        project_tail(1, 2)
-        hand(2, 3)
+        project_conv(2, f, True, 1 - head_b)
+        project_conv(2, f, False, head_b)
+        mix(2, f, False, "head")
+        conv_return(2, True, False, "head").start()
+        project_conv(2, f, False, 1 - head_b)
+        mix(2, f, False, "tail")
+        conv_return(2, True, False, "tail").start()
+        project_conv(2, f, True, head_b)
+        pr_start(2, f, 0)
+        hand(2, 2)
         conv_own(2, False)
         project_conv(2, other, False, head_b)
         conv_end_close(2, "head")
-        conv_close(2, False)
         have(5, 2)
+        project_tail(1, 2)
+        hand(2, 3)
+        project_tail(2, 2)
+        have(6, 2)
         project_tail(1, 3)
         conv_end_close(1, "tail")
-        project_tail(2, 2)
         project_tail(2, 3)
         conv_end_close(2, "tail")
+        conv_close(2, False)
         conv_close(2, True)
         for g in (1, 2):
             conv_return(g, False, True).wait_recv()
             conv_return(g, True, True).wait()
             conv_return(g, False, True).wait_send()
-            conv_return(g, True, False).wait_send()
+            for span in (None,) if g == 1 else ("head", "tail"):
+                conv_return(g, True, False, span).wait_send()
             conv_return(g, False, False, "head").wait_send()
             conv_return(g, False, False, "tail").wait_send()
             pieces_sent(tok_t_send.at[g], 3 * SUBS if g == 1 else 3 * SUBS - Y_PAIRS)
@@ -930,6 +953,21 @@
     pieces_sent(tok_t_send.at[0], 3 * SUBS)
     for own in (True, False):
         finish(attn_return(own))
+
+
+def deliver(attended, conv, logs, attn_out, conv_out, log_out, log_buf, sems):
+    half = logs.shape[1]
+    copies = [
+        pltpu.make_async_copy(a, b, sems.at[i])
+        for i, (a, b) in enumerate(((attended, attn_out), (conv, conv_out), (log_buf, log_out)))
+    ]
+    copies[0].start()
+    copies[1].start()
+    for i in range(2):
+        log_buf[pl.ds(i * half, half), :] = logs[i]
+    copies[2].start()
+    for c in copies:
+        c.wait()
 
 
 def fused_device(
@@ -998,15 +1036,15 @@
             dma((1,)),
             dma((3,)),
             dma((3, SUBS, 2)),
-            dma((6,)),
+            dma((7,)),
             dma((2, 2)),
             dma((2, 2)),
             dma((2, 2)),
             dma((2, 2)),
             dma((2,)),
             dma((2,)),
+            dma((2, 5)),
             dma((2, 4)),
-            dma((2, 3)),
         ],
         compiler_params=pltpu.CompilerParams(
             collective_id=0, has_side_effects=True, vmem_limit_bytes=48 << 20
@@ -1028,7 +1066,20 @@
             )
         )
     )
-    return (attended[None], conv[None], logs.reshape(1, head_local, rows))
+    vmem = pl.BlockSpec(memory_space=pltpu.VMEM)
+    attended, conv, logs = pl.pallas_call(
+        deliver,
+        out_shape=(
+            jax.ShapeDtypeStruct((rows, local), bf),
+            jax.ShapeDtypeStruct((rows, 4 * chans), bf),
+            jax.ShapeDtypeStruct((head_local, rows), f32),
+        ),
+        in_specs=[vmem] * 3,
+        out_specs=(hbm, hbm, hbm),
+        scratch_shapes=[pltpu.VMEM((head_local, rows), f32), dma((3,))],
+        compiler_params=pltpu.CompilerParams(vmem_limit_bytes=8 << 20),
+    )(attended, conv, logs)
+    return (attended[None], conv[None], logs[None])
 
 
 def fits(mesh, args):

time: 87.4 us -> 82.2 us (0.941)
  Pallas kernels: 84.2 us -> 81.3 us
  local copies, waits for them, and re-layouts: 2.38 us -> 0 us
    pallas_call x1, Pallas kernels: 84.2 us -> 80.1 us  [fused_device(): pl.pallas_call(functools.partial(mega_kernel, tps), out_shape=(jax.ShapeD...]
    unnamed x2 -> x0, local copies, waits for them, and re-layouts: 1.76 us -> none
    pallas_call x0 -> x1, Pallas kernels: none -> 1.17 us  [fused_device(): pl.pallas_call(deliver, out_shape=(jax.ShapeDtypeStruct((rows, local), bf...]
where the time goes in v6:
time: 82.2 us; the launch traced here: 82.1 us
  Pallas kernels  81.3 us (99%)
    pallas_call x1, Pallas kernels, fused_device(): pl.pallas_call(functools.partial(mega_kernel, tps), out_shape=(jax.ShapeD...  80.1 us

profile of v6, /device:TPU:0, one launch (start us, length us, event | category | flops | bytes accessed | tf_op | source)
XLA Modules:
  0.0 82.1 jit_solution(15864995181992754780)
XLA Ops:
  0.6 80.1 %shard_map.121 = (bf16[768,512]{1,0:T(8,128)(2,1)S(1)}, bf16[768,512]{1,0:T(8,128)(2,1)S(1)}, f32[2,4,768]{2,1,0:T(4,128)S(1)}) custom-call(bf16[768,2304]{1,0:T(8,128)(2,1)} %bitcast.5, f32[18,128]{1,0:T(8,128)} %bitcast.6, bf16[288,512]{1,0:T(8,128)(2,1)} %qw.1, bf16[288,128]{1,0:T(8,128)(2,1)} %kw.1, bf16[288,128]{1,0:T(8,128)(2,1)} %vw.1, ...), custom_call_target="tpu_custom_call" | custom-call | tf_op jit(solution)/shard_map/pallas_call | solution.py:998
  80.7 1.2 %shard_map.122 = (bf16[768,512]{1,0:T(8,128)(2,1)}, bf16[768,512]{1,0:T(8,128)(2,1)}, f32[8,768]{1,0:T(8,128)}) custom-call(bf16[768,512]{1,0:T(8,128)(2,1)S(1)} %get-tuple-element.9.attended, bf16[768,512]{1,0:T(8,128)(2,1)S(1)} %get-tuple-element.10.conv, f32[2,4,768]{2,1,0:T(4,128)S(1)} %get-tuple-element.11.logs), custom_call_target="tpu_custom_call" | custom-call | tf_op jit(solution)/shard_map/pallas_call | solution.py:1070

commit v7 on v6

--- a/solution.py
+++ b/solution.py
@@ -584,6 +584,8 @@
         None: (0, rows),
         "head": (jnp.where(low_half, rows - split, 0), split),
         "tail": (jnp.where(low_half, 0, split), rows - split),
+        "far": (jnp.where(low_half, 0, rows - split), split),
+        "rest": (jnp.where(low_half, split, 0), rows - split),
     }
 
     def conv_return(g, own_seq, own_rows, span=None):
@@ -595,7 +597,7 @@
         if own_seq and own_rows:
             return pltpu.make_async_copy(src, dst, own_sem.at[g - 1])
         if own_seq:
-            last = 3 if span == "tail" else 0
+            last = 3 if span == "rest" else 0
             return remote(src, dst, conv_send.at[g - 1, last], conv_recv.at[g - 1, last], pair)
         if own_rows:
             return remote(src, dst, conv_send.at[g - 1, 1], conv_recv.at[g - 1, 1], across)
@@ -794,7 +796,7 @@
         attend(other, 0, 2, blocks - 1, True)
         begin(attn_return(False))
         for g in (1, 2):
-            for span in (None,) if g == 1 else ("head", "tail"):
+            for span in (None,) if g == 1 else ("far", "rest"):
                 conv_return(g, True, False, span).wait_recv()
             conv_return(g, False, False, "head").wait_recv()
             conv_return(g, False, False, "tail").wait_recv()
@@ -893,11 +895,11 @@
         conv_close_end(1)
         near(2, f)
         near(2, other)
+        take(2, 3)
         near(2, 2 + f)
+        hand(2, 0)
         conv_close(1, True)
-        hand(2, 0)
         hand(2, 1)
-        take(2, 3)
         have(4, 4)
         near(1, 2 + other, head_b)
         project_conv(1, other, False, head_b)
@@ -906,35 +908,35 @@
         near(2, 2 + other, head_b)
         for blk in ct + ft:
             arrived(2, blk)
+        project_conv(2, f, False, 1 - head_b)
+        mix(2, f, False, "far")
+        conv_return(2, True, False, "far").start()
         project_conv(2, f, True, 1 - head_b)
         project_conv(2, f, False, head_b)
-        mix(2, f, False, "head")
-        conv_return(2, True, False, "head").start()
-        project_conv(2, f, False, 1 - head_b)
-        mix(2, f, False, "tail")
-        conv_return(2, True, False, "tail").start()
-        project_conv(2, f, True, head_b)
-        pr_start(2, f, 0)
+        mix(2, f, False, "rest")
+        conv_return(2, True, False, "rest").start()
         hand(2, 2)
         conv_own(2, False)
         project_conv(2, other, False, head_b)
         conv_end_close(2, "head")
+        hand(2, 3)
+        project_conv(2, f, True, head_b)
+        pr_start(2, f, 0)
         have(5, 2)
         project_tail(1, 2)
-        hand(2, 3)
-        project_tail(2, 2)
         have(6, 2)
         project_tail(1, 3)
         conv_end_close(1, "tail")
+        conv_close(2, False)
+        project_tail(2, 2)
         project_tail(2, 3)
         conv_end_close(2, "tail")
-        conv_close(2, False)
         conv_close(2, True)
         for g in (1, 2):
             conv_return(g, False, True).wait_recv()
             conv_return(g, True, True).wait()
             conv_return(g, False, True).wait_send()
-            for span in (None,) if g == 1 else ("head", "tail"):
+            for span in (None,) if g == 1 else ("far", "rest"):
                 conv_return(g, True, False, span).wait_send()
             conv_return(g, False, False, "head").wait_send()
             conv_return(g, False, False, "tail").wait_send()

time: 82.2 us -> 81.8 us (level)
  no operation moved by 1% of the time
where the time goes in v7:
time: 81.8 us; the launch traced here: 81.6 us
  Pallas kernels  80.8 us (99%)
  between operations  0.82 us (1%)
    pallas_call x1, Pallas kernels, fused_device(): pl.pallas_call(functools.partial(mega_kernel, tps), out_shape=(jax.ShapeD...  79.6 us

profile of v7, /device:TPU:0, one launch (start us, length us, event | category | flops | bytes accessed | tf_op | source)
XLA Modules:
  0.0 81.6 jit_solution(17823752295748331648)
XLA Ops:
  0.6 79.6 %shard_map.121 = (bf16[768,512]{1,0:T(8,128)(2,1)S(1)}, bf16[768,512]{1,0:T(8,128)(2,1)S(1)}, f32[2,4,768]{2,1,0:T(4,128)S(1)}) custom-call(bf16[768,2304]{1,0:T(8,128)(2,1)} %bitcast.5, f32[18,128]{1,0:T(8,128)} %bitcast.6, bf16[288,512]{1,0:T(8,128)(2,1)} %qw.1, bf16[288,128]{1,0:T(8,128)(2,1)} %kw.1, bf16[288,128]{1,0:T(8,128)(2,1)} %vw.1, ...), custom_call_target="tpu_custom_call" | custom-call | tf_op jit(solution)/shard_map/pallas_call | solution.py:1000
  80.3 1.2 %shard_map.122 = (bf16[768,512]{1,0:T(8,128)(2,1)}, bf16[768,512]{1,0:T(8,128)(2,1)}, f32[8,768]{1,0:T(8,128)}) custom-call(bf16[768,512]{1,0:T(8,128)(2,1)S(1)} %get-tuple-element.9.attended, bf16[768,512]{1,0:T(8,128)(2,1)S(1)} %get-tuple-element.10.conv, f32[2,4,768]{2,1,0:T(4,128)S(1)} %get-tuple-element.11.logs), custom_call_target="tpu_custom_call" | custom-call | tf_op jit(solution)/shard_map/pallas_call | solution.py:1072

commit v8 on v7

--- a/solution.py
+++ b/solution.py
@@ -324,27 +324,38 @@
             device_id_type=MESH,
         )
 
+    def arrive_sem(g, blk, crosses=False):
+        if g == 0:
+            return w_recv.at[blk]
+        if crosses:
+            return w_recv.at[4 * SPAN + g - 1]
+        return w_recv.at[2 * SPAN + SPAN * (g - 1) + lax.rem(blk, SPAN)]
+
     def y_copy(g):
         return remote(
-            stage_w.at[g], wts.at[g, block_rows(mine)], y_send.at[g], w_recv.at[g, mine], across
-        )
-
-    def block_copy(g, blk, send, peer):
+            stage_w.at[g], wts.at[g, block_rows(mine)], y_send.at[0], arrive_sem(g, mine), across
+        )
+
+    def block_copy(g, blk, send, peer, crosses=False):
         at = wts.at[g, block_rows(blk)]
-        return remote(at, at, send, w_recv.at[g, blk], peer)
+        return remote(at, at, send, arrive_sem(g, blk, crosses), peer)
 
     def to_pair(g, blk):
         return block_copy(g, blk, pair_send.at[0], pair)
 
     def to_mid(g, blk):
-        return block_copy(g, blk, mid_send.at[g], mid)
+        return block_copy(g, blk, mid_send.at[0], mid, True)
 
     def blocks_sent(send, count):
         at = wts.at[0, pl.ds(0, count * depth)]
-        remote(at, at, send, w_recv.at[0, 0], across).wait_send()
+        remote(at, at, send, w_recv.at[0], across).wait_send()
 
     def arrived(g, blk):
         to_pair(g, blk).wait_recv()
+
+    def far_arrived(g):
+        at = wts.at[g, pl.ds(0, SPAN * depth)]
+        remote(at, at, mid_send.at[0], arrive_sem(g, 0, True), mid).wait_recv()
 
     def slot_of(k):
         return (other, 2 + f, 2 + other)[k]
@@ -598,12 +609,12 @@
             return pltpu.make_async_copy(src, dst, own_sem.at[g - 1])
         if own_seq:
             last = 3 if span == "rest" else 0
-            return remote(src, dst, conv_send.at[g - 1, last], conv_recv.at[g - 1, last], pair)
+            return remote(src, dst, conv_send.at[g - 1], conv_recv.at[g - 1, last], pair)
         if own_rows:
-            return remote(src, dst, conv_send.at[g - 1, 1], conv_recv.at[g - 1, 1], across)
+            return remote(src, dst, conv_send.at[g - 1], conv_recv.at[g - 1, 1], across)
         last = 1 if span == "tail" else 0
         return remote(
-            src, dst, conv_send.at[g - 1, 2 + 2 * last], conv_recv.at[g - 1, 1 + last], diag
+            src, dst, conv_send.at[g - 1], conv_recv.at[g - 1, 1 + last], diag
         )
 
     def project_conv(g, seq, own_rows, only=None):
@@ -868,8 +879,7 @@
         near(1, other)
         relay(2, theirs, to_mid)
         take(1, 3)
-        for blk in ct + ft:
-            arrived(1, blk)
+        far_arrived(1)
         conv_own(1, True)
         conv_own(1, False)
         kv_wait(f, 0)
@@ -906,8 +916,7 @@
         conv_end_close(1, "head")
         conv_close(1, False)
         near(2, 2 + other, head_b)
-        for blk in ct + ft:
-            arrived(2, blk)
+        far_arrived(2)
         project_conv(2, f, False, 1 - head_b)
         mix(2, f, False, "far")
         conv_return(2, True, False, "far").start()
@@ -935,22 +944,18 @@
         for g in (1, 2):
             conv_return(g, False, True).wait_recv()
             conv_return(g, True, True).wait()
-            conv_return(g, False, True).wait_send()
-            for span in (None,) if g == 1 else ("far", "rest"):
-                conv_return(g, True, False, span).wait_send()
-            conv_return(g, False, False, "head").wait_send()
-            conv_return(g, False, False, "tail").wait_send()
+            sent = conv_st.at[0, :, pl.ds(0, 3 * rows // 2)]
+            remote(sent, sent, conv_send.at[g - 1], conv_recv.at[g - 1, 1], across).wait_send()
             pieces_sent(tok_t_send.at[g], 3 * SUBS if g == 1 else 3 * SUBS - Y_PAIRS)
         blocks_sent(pair_send.at[0], 6)
-        for g in range(GROUPS):
-            blocks_sent(mid_send.at[g], 4)
+        sent = wts.at[pl.ds(0, 2), pl.ds(0, 2 * GROUPS * depth)]
+        remote(sent, sent, mid_send.at[0], w_recv.at[0], across).wait_send()
         pieces_sent(tok_y_send.at[1], Z_FIRST + Y_PAIRS)
 
     pl.when(is_end)(end_program)
     pl.when(is_mid)(mid_program)
 
-    for g in range(GROUPS):
-        y_copy(g).wait_send()
+    blocks_sent(y_send.at[0], GROUPS)
     pieces_sent(tok_y_send.at[0], SUBS)
     pieces_sent(tok_t_send.at[0], 3 * SUBS)
     for own in (True, False):
@@ -1030,10 +1035,10 @@
             dma((GROUPS,)),
             dma((3,)),
             dma((2,)),
-            dma((GROUPS,)),
-            dma((GROUPS, 2 * SPAN)),
             dma((1,)),
-            dma((GROUPS,)),
+            dma((4 * SPAN + GROUPS - 1,)),
+            dma((1,)),
+            dma((1,)),
             dma((2,)),
             dma((1,)),
             dma((3,)),
@@ -1045,7 +1050,7 @@
             dma((2, 2)),
             dma((2,)),
             dma((2,)),
-            dma((2, 5)),
+            dma((2,)),
             dma((2, 4)),
         ],
         compiler_params=pltpu.CompilerParams(

time: 81.8 us -> 81.6 us (level)
  no operation moved by 1% of the time
where the time goes in v8:
time: 81.6 us; the launch traced here: 81.5 us
  Pallas kernels  80.6 us (99%)
  between operations  0.82 us (1%)
    pallas_call x1, Pallas kernels, fused_device(): pl.pallas_call(functools.partial(mega_kernel, tps), out_shape=(jax.ShapeD...  79.5 us

profile of v8, /device:TPU:0, one launch (start us, length us, event | category | flops | bytes accessed | tf_op | source)
XLA Modules:
  0.0 81.5 jit_solution(12552274734662601748)
XLA Ops:
  0.6 79.5 %shard_map.121 = (bf16[768,512]{1,0:T(8,128)(2,1)S(1)}, bf16[768,512]{1,0:T(8,128)(2,1)S(1)}, f32[2,4,768]{2,1,0:T(4,128)S(1)}) custom-call(bf16[768,2304]{1,0:T(8,128)(2,1)} %bitcast.5, f32[18,128]{1,0:T(8,128)} %bitcast.6, bf16[288,512]{1,0:T(8,128)(2,1)} %qw.1, bf16[288,128]{1,0:T(8,128)(2,1)} %kw.1, bf16[288,128]{1,0:T(8,128)(2,1)} %vw.1, ...), custom_call_target="tpu_custom_call" | custom-call | tf_op jit(solution)/shard_map/pallas_call | solution.py:1005
  80.1 1.2 %shard_map.122 = (bf16[768,512]{1,0:T(8,128)(2,1)}, bf16[768,512]{1,0:T(8,128)(2,1)}, f32[8,768]{1,0:T(8,128)}) custom-call(bf16[768,512]{1,0:T(8,128)(2,1)S(1)} %get-tuple-element.9.attended, bf16[768,512]{1,0:T(8,128)(2,1)S(1)} %get-tuple-element.10.conv, f32[2,4,768]{2,1,0:T(4,128)S(1)} %get-tuple-element.11.logs), custom_call_target="tpu_custom_call" | custom-call | tf_op jit(solution)/shard_map/pallas_call | solution.py:1077
